TPU v7x, 512 devices: a whole 4x8x8 slice. The times are simulated.
512 devices in a mesh: sp: 64 (over z, y), fs: 4 (over x), tp: 2 (over core).
Axes of the slice: x: 4, y: 8, z: 8, core: 2. Of those that a mesh axis runs over, the one named last changes fastest.
Arguments:
- tokens: bfloat16 [65536, 2048], P(('fs', 'sp')), parts along dimension 0, may hold values from -6 to 6
- norm_gain: float32 [2048], replicated, may hold values from 0.1 to 1.9
- w_query: bfloat16 [2048, 1024], P('sp', 'tp'), may hold values from -0.080939698 to 0.080939698
- w_key: bfloat16 [2048, 256], P('sp', 'tp'), may hold values from -0.080939698 to 0.080939698
- w_value: bfloat16 [2048, 256], P('sp', 'tp'), may hold values from -0.125 to 0.125
- w_conv_in: bfloat16 [2048, 1024], P('sp', 'tp'), may hold values from -0.125 to 0.125
- w_conv_gate: bfloat16 [2048, 1024], P('sp', 'tp'), may hold values from -0.125 to 0.125
- sink_logit: float32 [16], P('tp'), may hold values from 2 to 6
- conv_taps: float32 [31, 1024], P(None, 'tp'), may hold values from -5.3881591 to 5.3881591
- conv_bias: float32 [1024], P('tp'), may hold values from -0.9 to 5.9
- channel_gain: float32 [1024], P('tp'), may hold values from 0.1 to 1.9
- channel_shift: float32 [1024], P('tp'), may hold values from -3 to 3
- w_attn_out: bfloat16 [1024, 2048], P(None, 'sp'), may hold values from -1.5 to 1.5
- w_conv_out: bfloat16 [1024, 2048], P(None, 'sp'), may hold values from -0.1875 to 0.1875
Outputs:
- output: bfloat16 [65536, 2048], P(('fs', 'sp', 'tp')), parts along dimension 0
There are 4 independent parts, one for each index of `fs`. A program takes and returns all parts, laid end to end along the dimension named above; an argument that names none is the same for every part. Nothing has to cross between parts.
All inputs are finite; a program needn't handle non-finite values.
Results may differ from a plain program's by a relative error of at most 0.011.
Values may be sent and summed in bfloat16 or wider, within the bound.
A program may use at most 64 MiB of HBM per device.

v0:
```python
import jax
import jax.numpy as jnp
from jax import lax
from jax.sharding import PartitionSpec as P

HEAD_DIM = 64
WINDOW = 128
GRID_W = 64


EPSILON = 1e-06
NEGATIVE = -1e30
ROPE_BASE = 10000.0


def in_one_piece(arrays, axis, dim, along):
    widths = [a.shape[along] for a in arrays]
    both = jnp.concatenate(arrays, axis=along)
    result = lax.all_gather(both, axis, axis=dim, tiled=True)
    return tuple(jnp.split(result, [sum(widths[:k]) for k in range(1, len(widths))], axis=along))


def padded(block, sides, width):
    for axis, dim in sides:
        count = lax.axis_size(axis)
        forward = [(i, i + 1) for i in range(count - 1)]
        backward = [(target, source) for source, target in forward]
        low = lax.ppermute(
            lax.slice_in_dim(block, block.shape[dim] - width, None, axis=dim), axis, forward
        )
        high = lax.ppermute(lax.slice_in_dim(block, 0, width, axis=dim), axis, backward)
        block = jnp.concatenate([low, block, high], axis=dim)
    return block


def over_pieces(array, axis):
    return lax.all_gather(array, axis).sum(0)


def cut_along(array, dim, count):
    before, after = (array.shape[:dim], array.shape[dim + 1 :])
    return jnp.moveaxis(array.reshape(*before, count, -1, *after), dim, 0)


def sum_at_owner(array, axis, dim):
    count = lax.axis_size(axis)
    parts = lax.all_to_all(cut_along(array, dim, count), axis, 0, 0, tiled=True)
    return jnp.sum(parts.astype(jnp.float32), axis=0)


def rotate_pairs(values, positions):
    middle = values.shape[-1] // 2
    inverse = ROPE_BASE ** (-jnp.arange(middle, dtype=jnp.float32) / middle)
    angles = positions.astype(jnp.float32)[:, None] * inverse[None, :]
    cosine = jnp.cos(angles)[:, None, :]
    sine_table = jnp.sin(angles)[:, None, :]
    leading = values[..., :middle]
    trailing = values[..., middle:]
    return jnp.concatenate(
        [leading * cosine - trailing * sine_table, leading * sine_table + trailing * cosine],
        axis=-1,
    )


def grid_rotate(values, positions):
    middle = values.shape[-1] // 2
    return jnp.concatenate(
        [
            rotate_pairs(values[..., :middle], positions // GRID_W),
            rotate_pairs(values[..., middle:], positions % GRID_W),
        ],
        axis=-1,
    )


def local(
    tokens,
    norm_gain,
    w_query,
    w_key,
    w_value,
    w_conv_in,
    w_conv_gate,
    sink_logit,
    conv_taps,
    conv_bias,
    channel_gain,
    channel_shift,
    w_attn_out,
    w_conv_out,
):
    rows_here = tokens.shape[0]
    offset = lax.axis_index("sp") * rows_here
    total = rows_here * lax.axis_size("sp")
    tp_count = lax.axis_size("tp")
    token_float = tokens.astype(jnp.float32)
    normed = (
        token_float
        * lax.rsqrt(jnp.mean(token_float * token_float, axis=-1, keepdims=True) + EPSILON)
        * norm_gain[None, :]
    ).astype(jnp.bfloat16)
    head_cols = w_query.shape[1]
    kv_cols = w_key.shape[1]
    chan_cols = w_conv_in.shape[1]
    piece_query, piece_key, piece_value, piece_conv, piece_gate = in_one_piece(
        (w_query, w_key, w_value, w_conv_in, w_conv_gate), "sp", 0, 1
    )
    query_acc = jnp.dot(normed, piece_query, preferred_element_type=jnp.float32)
    pair_acc = jnp.dot(
        normed,
        jnp.concatenate([piece_key, piece_value], axis=1),
        preferred_element_type=jnp.float32,
    )
    conv_acc = jnp.dot(
        normed,
        jnp.concatenate([piece_conv, piece_gate], axis=1),
        preferred_element_type=jnp.float32,
    )
    positions = offset + jnp.arange(rows_here, dtype=jnp.int32)
    heads_here = head_cols // HEAD_DIM
    kv_here = kv_cols // HEAD_DIM
    group = heads_here // kv_here
    query = grid_rotate(query_acc.reshape(rows_here, heads_here, HEAD_DIM), positions).astype(
        jnp.bfloat16
    )
    keys = grid_rotate(pair_acc[:, :kv_cols].reshape(rows_here, kv_here, HEAD_DIM), positions)
    keys = keys.astype(jnp.bfloat16).reshape(rows_here, kv_cols)
    values = pair_acc[:, kv_cols:].astype(jnp.bfloat16)
    stacked = jnp.concatenate([keys, values], axis=1)
    extended = padded(stacked, (("sp", 0),), WINDOW)
    block = min(rows_here, 512)
    span = block + 2 * WINDOW
    sinks = sink_logit.reshape(kv_here, group)[:, :, None, None]
    queries = query.reshape(block, kv_here, group, HEAD_DIM)
    near_keys = extended[:, :kv_cols].reshape(span, kv_here, HEAD_DIM)
    near_values = extended[:, kv_cols:].reshape(span, kv_here, HEAD_DIM)
    scores = jnp.einsum(
        "qkgd,skd->kgqs", queries, near_keys, preferred_element_type=jnp.float32
    ) * HEAD_DIM ** (-0.5)
    query_pos = offset + 0 + jnp.arange(block, dtype=jnp.int32)
    key_pos = offset + 0 - WINDOW + jnp.arange(span, dtype=jnp.int32)
    valid = (
        (jnp.abs(query_pos[:, None] - key_pos[None, :]) <= WINDOW)
        & (key_pos[None, :] >= 0)
        & (key_pos[None, :] < total)
    )
    scores = jnp.where(valid[None, None], scores, NEGATIVE)
    top = jnp.maximum(jnp.max(scores, axis=-1, keepdims=True), sinks)
    raised = jnp.exp(scores - top)
    denominator = jnp.sum(raised, axis=-1, keepdims=True) + jnp.exp(sinks - top)
    probs = (raised / denominator).astype(jnp.bfloat16)
    mixed = jnp.einsum("kgqs,skd->qkgd", probs, near_values, preferred_element_type=jnp.float32)
    outputs = mixed.astype(jnp.bfloat16).reshape(block, head_cols)
    glu = (conv_acc[:, :chan_cols] * jax.nn.sigmoid(conv_acc[:, chan_cols:])).astype(jnp.bfloat16)
    reach = conv_taps.shape[0] // 2
    rims = padded(glu, (("sp", 0),), reach)
    filtered = jnp.zeros((rows_here, chan_cols), jnp.float32) + conv_bias[None, :]
    for shift_index in range(conv_taps.shape[0]):
        filtered = filtered + conv_taps[shift_index][None, :] * rims[
            shift_index : shift_index + rows_here
        ].astype(jnp.float32)
    channel_total = chan_cols * tp_count
    first_sum, square_sum = (
        over_pieces(jnp.sum(filtered, axis=-1), "tp"),
        over_pieces(jnp.sum(filtered * filtered, axis=-1), "tp"),
    )
    centre = first_sum[:, None] / channel_total
    centred = filtered - centre
    spread = square_sum[:, None] / channel_total - centre * centre
    conv_out = jax.nn.silu(
        centred * lax.rsqrt(spread + EPSILON) * channel_gain[None, :] + channel_shift[None, :]
    ).astype(jnp.bfloat16)
    features = jnp.concatenate([outputs, conv_out], axis=1)
    tp_here = lax.axis_index("tp")
    own_rows = jnp.concatenate(
        [
            lax.dynamic_slice_in_dim(w_attn_out, tp_here * head_cols, head_cols, 0),
            lax.dynamic_slice_in_dim(w_conv_out, tp_here * chan_cols, chan_cols, 0),
        ],
        axis=0,
    )
    own_whole = lax.all_gather(own_rows, "sp", axis=1, tiled=True)
    result = sum_at_owner(
        jnp.dot(features, own_whole, preferred_element_type=jnp.float32).astype(jnp.bfloat16),
        "tp",
        0,
    )
    return result.astype(jnp.bfloat16)


def solution(mesh):
    in_specs = (
        P(("fs", "sp"), None),
        P(),
        P("sp", "tp"),
        P("sp", "tp"),
        P("sp", "tp"),
        P("sp", "tp"),
        P("sp", "tp"),
        P("tp"),
        P(None, "tp"),
        P("tp"),
        P("tp"),
        P("tp"),
        P(None, "sp"),
        P(None, "sp"),
    )
    out_specs = P(("fs", "sp", "tp"), None)
    return jax.shard_map(local, mesh=mesh, in_specs=in_specs, out_specs=out_specs, check_vma=False)
```

profile of v0, /device:TPU:1, one launch (start us, length us, event | category | flops | bytes accessed | tf_op | source)
XLA Modules:
  0.0 215.0 jit_solution(4351663836033229892)
XLA Ops:
  6.5 0.0 copy-start
  6.5 0.0 copy-start.5
  6.5 0.0 all-gather.7.cloned.1.call-start
  6.5 0.8 constant_dynamic-update-slice_fusion.4
  7.4 0.7 constant_dynamic-update-slice_fusion.3
  8.1 0.7 constant_dynamic-update-slice_fusion.2
  8.8 0.8 constant_dynamic-update-slice_fusion.1
  9.6 0.8 constant_dynamic-update-slice_fusion
  10.3 0.0 copy-start.1
  10.3 0.6 copy-done.1
  11.0 0.0 all-gather.7.cloned.1.call-update
  11.0 0.0 all-gather.9.cloned.1.call-start
  11.0 0.8 constant_dynamic-slice_fusion
  11.8 0.6 pad_maximum_fusion.5
  12.5 0.0 all-gather.9.cloned.1.call-update
  12.5 0.7 max.18
  13.3 1.5 fusion.4
  14.8 1.0 fusion.76
  15.8 1.2 fusion.75
  17.0 0.2 multiply_cosine_fusion.1
  17.2 0.3 fusion.22
  17.5 93.4 %all-gather.7.cloned.1.call-done = bf16[2048,1792]{1,0:T(8,128)(2,1)} async-done(((bf16[32,1792]{1,0:T(8,128)(2,1)}), bf16[2048,1792]{1,0:T(8,128)(2,1)}) %all-gather.7.cloned.1.call-update) | async-done | bytes 7340048 | tf_op jit(solution)/shard_map/all_gather | solution.py:19
  110.9 2.2 %fusion.11 = f32[256,256]{0,1:T(8,128)S(1)} fusion(bf16[2048,1792]{1,0:T(8,128)(2,1)} %all-gather.7.cloned.1.call-done, bf16[256,2048]{1,0:T(8,128)(2,1)} %param.14, f32[2048]{0:T(1024)} %param.15, f32[256]{0:T(256)S(1)} %add_rsqrt_fusion.1), kind=kOutput, calls=%fused_computation.45 | convolution fusion | flops 270532608 | bytes 2368512 | tf_op jit(solution)/shard_map/dot_general | solution.py:109
  113.2 2.7 %collective-permute-start = (bf16[128,256]{0,1:T(8,128)(2,1)S(1)}, bf16[128,256]{0,1:T(8,128)(2,1)S(1)}, u32[]{:S(2)}, u32[]{:S(2)}) collective-permute-start(bf16[128,256]{0,1:T(8,128)(2,1)S(1)} %get-tuple-element.22), channel_id=1, source_target_pairs={{0,8},{8,16},{16,24},{24,32},{32,40},{40,48},{48,56},{56,64},{64,7... | collective-permute-start | bytes 196616 | tf_op jit(solution)/shard_map/ppermute | solution.py:28
  115.9 1.3 collective-permute-start.1
  117.2 0.0 copy-done
  117.2 0.0 copy-done.5
  117.2 3.5 %fusion = f32[256,1024]{1,0:T(8,128)S(1)} fusion(bf16[2048,1792]{1,0:T(8,128)(2,1)} %all-gather.7.cloned.1.call-done, bf16[256,2048]{1,0:T(8,128)(2,1)S(1)} %copy-done, f32[2048]{0:T(1024)S(1)} %copy-done.5, f32[256]{0:T(256)S(1)} %add_rsqrt_fusion.1), kind=kOutput, calls=%fused_computation | convolution fusion | flops 1075838976 | bytes 6300672 | tf_op jit(solution)/shard_map/dot_general | solution.py:114
  120.7 0.0 copy-start.2
  120.7 0.0 copy-start.3
  120.7 0.0 copy-start.4
  120.8 0.1 fusion.20
  120.9 4.0 %collective-permute-start.2 = (bf16[15,512]{1,0:T(8,128)(2,1)S(1)}, bf16[15,512]{1,0:T(8,128)(2,1)S(1)}, u32[]{:S(2)}, u32[]{:S(2)}) collective-permute-start(bf16[15,512]{1,0:T(8,128)(2,1)S(1)} %get-tuple-element.16), channel_id=1, source_target_pairs={{0,8},{8,16},{16,24},{24,32},{32,40},{40,48},{48,56},{56,64},{64,7... | collective-permute-start | bytes 46088 | tf_op jit(solution)/shard_map/ppermute | solution.py:28
  124.9 1.3 collective-permute-start.3
  126.2 2.6 %fusion.7 = f32[256,512]{0,1:T(8,128)S(1)} fusion(bf16[2048,1792]{1,0:T(8,128)(2,1)} %all-gather.7.cloned.1.call-done, bf16[256,2048]{1,0:T(8,128)(2,1)S(1)} %copy-done, f32[2048]{0:T(1024)S(1)} %copy-done.5, f32[256]{0:T(256)S(1)} %add_rsqrt_fusion.1), kind=kOutput, calls=%fused_computation.13 | convolution fusion | flops 538968064 | bytes 3679232 | tf_op jit(solution)/shard_map/dot_general | solution.py:108
  128.9 0.1 subtract_convert_fusion.1
  129.0 0.0 collective-permute-done.2
  129.0 0.4 collective-permute-done.3
  129.4 0.0 copy-done.2
  129.4 3.1 %fusion.72 = (f32[256]{0:T(256)S(1)}, f32[256]{0:T(256)S(1)}, f32[256,512]{1,0:T(8,128)S(1)}) fusion(bf16[15,512]{1,0:T(8,128)(2,1)S(1)} %collective-permute-done.3, bf16[256,512]{1,0:T(8,128)(2,1)S(1)} %fusion.20, f32[512]{0:T(512)S(1)} %bitcast.90, f32[512]{0:T(512)S(1)} %bitcast.91, f32[512]{0:T(512)S(1)} %bitcast.93, f32[512]{0:T(512)S(1)} %bitcast.94, ...), kind=kLoop, calls=%fused_computation.167 | loop fusion | flops 24378880 | bytes 884736 | tf_op jit(solution)/shard_map/reduce_sum | solution.py:164
  132.5 4.3 %all-gather.2 = f32[2,1,256]{2,1,0:T(1,128)S(1)} all-gather(f32[1,1,256]{2,1,0:T(1,128)S(1)} %bitcast.112), channel_id=2, replica_groups=mesh['sp'=64,'fs'=4,'tp'=2] {'tp'}, dimensions={0}, use_global_device_ids=true | all-gather | bytes 3072 | tf_op jit(solution)/shard_map/all_gather | solution.py:37
  136.8 1.8 all-gather.3
  138.6 0.0 copy-done.3
  138.6 0.0 copy-done.4
  138.6 0.3 multiply_convert_fusion
  138.9 0.0 collective-permute-done
  138.9 0.0 collective-permute-done.1
  139.0 0.8 fusion.3
  139.8 0.1 broadcast_maximum_fusion
  139.9 0.9 fusion.2
  140.8 0.1 exponential_add_fusion
  140.9 1.2 fusion.10
  142.1 0.1 copy.30
  142.2 52.3 %all-gather.9.cloned.1.call-done = bf16[1024,2048]{0,1:T(8,128)(2,1)} async-done(((bf16[1024,32]{0,1:T(8,128)(2,1)}), bf16[1024,2048]{0,1:T(8,128)(2,1)}) %all-gather.9.cloned.1.call-update) | async-done | bytes 4194320 | tf_op jit(solution)/shard_map/all_gather | solution.py:182
  194.5 3.5 %convolution_convert_fusion = bf16[256,2048]{1,0:T(8,128)(2,1)S(1)} fusion(bf16[1024,2048]{0,1:T(8,128)(2,1)} %all-gather.9.cloned.1.call-done, bf16[256,512]{1,0:T(8,128)(2,1)S(1)} %multiply_convert_fusion, bf16[256,512]{1,0:T(8,128)(2,1)S(1)} %copy.30), kind=kOutput, calls=%fused_computation.9 | convolution fusion | flops 1075314688 | bytes 5767168 | tf_op jit(solution)/shard_map/dot_general | solution.py:184
  198.0 9.0 %all_to_all.5 = bf16[2,128,2048]{2,1,0:T(8,128)(2,1)S(1)} all-to-all(bf16[2,128,2048]{2,1,0:T(8,128)(2,1)S(1)} %bitcast.68), channel_id=1, replica_groups=mesh['sp'=64,'fs'=4,'tp'=2] {'tp'}, dimensions={0} | all-to-all | bytes 2097152 | tf_op jit(solution)/shard_map/all_to_all | solution.py:47
  207.0 1.1 reduce_sum.72
  (17 shorter events, 0.2 us)
Async XLA Ops:
  6.5 110.7 %copy-start = (bf16[256,2048]{1,0:T(8,128)(2,1)S(1)}, bf16[256,2048]{1,0:T(8,128)(2,1)}, u32[]{:S(2)}) copy-start(bf16[256,2048]{1,0:T(8,128)(2,1)} %param.14) | copy-start | bytes 3145732
  6.5 110.7 %copy-start.5 = (f32[2048]{0:T(1024)S(1)}, f32[2048]{0:T(1024)}, u32[]{:S(2)}) copy-start(f32[2048]{0:T(1024)} %param.15) | copy-start | bytes 24580
  6.5 104.3 %all-gather.7.cloned.1.call-start = ((), (), s32[]{:S(2)}) async-start(), calls=%async_computation.1 | async-start | bytes 7454720 | tf_op jit(solution)/shard_map/all_gather | solution.py:19
  10.3 0.6 copy-start.1
  11.0 183.5 %all-gather.9.cloned.1.call-start = ((), (), s32[]{:S(2)}) async-start(), calls=%async_computation.2 | async-start | bytes 4259840 | tf_op jit(solution)/shard_map/all_gather | solution.py:182
  113.2 25.7 %collective-permute-start = (bf16[128,256]{0,1:T(8,128)(2,1)S(1)}, bf16[128,256]{0,1:T(8,128)(2,1)S(1)}, u32[]{:S(2)}, u32[]{:S(2)}) collective-permute-start(bf16[128,256]{0,1:T(8,128)(2,1)S(1)} %get-tuple-element.22), channel_id=1, source_target_pairs={{0,8},{8,16},{16,24},{24,32},{32,40},{40,48},{48,56},{56,64},{64,7... | collective-permute-start | bytes 196616 | tf_op jit(solution)/shard_map/ppermute | solution.py:28
  115.9 23.0 %collective-permute-start.1 = (bf16[128,256]{0,1:T(8,128)(2,1)S(1)}, bf16[128,256]{0,1:T(8,128)(2,1)S(1)}, u32[]{:S(2)}, u32[]{:S(2)}) collective-permute-start(bf16[128,256]{0,1:T(8,128)(2,1)S(1)} %get-tuple-element.23), channel_id=1, source_target_pairs={{8,0},{16,8},{24,16},{32,24},{40,32},{48,40},{56,48},{64,56},{72,6... | collective-permute-start | bytes 196616 | tf_op jit(solution)/shard_map/ppermute | solution.py:31
  120.7 8.7 %copy-start.2 = (f32[512]{0:T(512)S(1)}, f32[512]{0:T(512)}, u32[]{:S(2)}) copy-start(f32[512]{0:T(512)} %param.23) | copy-start | bytes 6148
  120.7 17.9 %copy-start.3 = (f32[512]{0:T(512)S(1)}, f32[512]{0:T(512)}, u32[]{:S(2)}) copy-start(f32[512]{0:T(512)} %param.25) | copy-start | bytes 6148
  120.7 17.9 %copy-start.4 = (f32[512]{0:T(512)S(1)}, f32[512]{0:T(512)}, u32[]{:S(2)}) copy-start(f32[512]{0:T(512)} %param.24) | copy-start | bytes 6148
  120.9 8.1 %collective-permute-start.2 = (bf16[15,512]{1,0:T(8,128)(2,1)S(1)}, bf16[15,512]{1,0:T(8,128)(2,1)S(1)}, u32[]{:S(2)}, u32[]{:S(2)}) collective-permute-start(bf16[15,512]{1,0:T(8,128)(2,1)S(1)} %get-tuple-element.16), channel_id=1, source_target_pairs={{0,8},{8,16},{16,24},{24,32},{32,40},{40,48},{48,56},{56,64},{64,7... | collective-permute-start | bytes 46088 | tf_op jit(solution)/shard_map/ppermute | solution.py:28
  124.9 4.5 %collective-permute-start.3 = (bf16[15,512]{1,0:T(8,128)(2,1)S(1)}, bf16[15,512]{1,0:T(8,128)(2,1)S(1)}, u32[]{:S(2)}, u32[]{:S(2)}) collective-permute-start(bf16[15,512]{1,0:T(8,128)(2,1)S(1)} %get-tuple-element.17), channel_id=1, source_target_pairs={{8,0},{16,8},{24,16},{32,24},{40,32},{48,40},{56,48},{64,56},{72,6... | collective-permute-start | bytes 46088 | tf_op jit(solution)/shard_map/ppermute | solution.py:31
Sparse Core Ops, SparseCore 0:
  11.1 99.7 all-gather.6
  113.9 80.5 all-gather.8
where the time goes:
time: 216 us; the launch traced here: 215 us
  waiting for transfers between devices  146 us (68%)
  blocking collectives  15.1 us (7%)
  matrix products  13.8 us (6%)
  between operations  13.7 us (6%)
  starting transfers between devices  9.34 us (4%)
  other arithmetic  8.51 us (4%)
  local copies, waits for them, and re-layouts  8.34 us (4%)
    all_gather x1, waiting for transfers between devices, in_one_piece(): result = lax.all_gather(both, axis, axis=dim, tiled=True)  93.4 us
    all_gather x1, waiting for transfers between devices, local(): own_whole = lax.all_gather(own_rows, 'sp', axis=1, tiled=True)  52.3 us
    all_to_all x1, blocking collectives, sum_at_owner(): parts = lax.all_to_all(cut_along(array, dim, count), axis, 0, 0, tiled=True)  9.02 us
    ppermute x2, starting transfers between devices, padded(): lax.ppermute(lax.slice_in_dim(block, block.shape[dim] - width, None, axis...  6.71 us
    all_gather x2, blocking collectives, over_pieces(): return lax.all_gather(array, axis).sum(0)  6.08 us
  transfers between devices with their start and end apart: 6, of which 3 were waited for; matrix products, arithmetic and copies ran while one was open for 10% of the time, Pallas kernels for 0%

commit v1 on v0

v1 whole, which is shorter than its diff:
```python
import functools
import math

import jax
import jax.numpy as jnp
from jax import lax
from jax.experimental import pallas as pl
from jax.experimental.pallas import tpu as pltpu
from jax.sharding import PartitionSpec as P

HEAD_DIM = 64
WINDOW = 128
EPSILON = 1e-06
NEGATIVE = -1e30
ROPE_BASE = 10000.0
TOK = 256
HALF = 128
D = 2048
TAPS = 31
RING = 8
FS = 4
CHUNK = 512
MESH = pl.DeviceIdType.MESH
NT = (((1,), (1,)), ((), ()))
F32 = jnp.float32
BF16 = jnp.bfloat16


def kernel(
    tokens_ref,
    gain_ref,
    wq_ref,
    wk_ref,
    wv_ref,
    wc_ref,
    wg_ref,
    sink_ref,
    taps_ref,
    bias_ref,
    cgain_ref,
    cshift_ref,
    wao_ref,
    wco_ref,
    out_ref,
    tok,
    win,
    wout,
    ctab,
    stab,
    qbuf,
    kvg,
    gext,
    low,
    high,
    sbuf,
    feat,
    raw,
    cvals,
    stat_out,
    stat_in,
    part,
    part_out,
    part_in,
    in_recv,
    in_send_a,
    in_send_b,
    out_recv,
    out_send_a,
    out_send_b,
    tok_recv,
    tok_send,
    tok_fwd,
    tok_pair,
    halo_recv,
    halo_send,
    feat_recv,
    feat_send,
    stat_sem,
    part_recv,
    part_send,
):
    sp = lax.axis_index("sp")
    f = lax.axis_index("fs")
    c = lax.axis_index("tp")
    z, y = sp // RING, sp % RING
    me_a = (1 - c) * y + c * z
    me_b = (1 - c) * z + c * y
    partner = 1 - c

    def sp_of(a, b):
        return (1 - c) * (b * RING + a) + c * (a * RING + b)

    def wrap(v):
        return (v + 2 * RING) % RING

    def fs_of(step):
        return (f + step) % FS

    has_low = sp > 0
    has_high = sp < RING * RING - 1

    barrier = pltpu.get_barrier_semaphore()

    def greet(**where):
        pl.semaphore_signal(barrier, inc=1, device_id=where, device_id_type=MESH)

    for step in range(1, RING):
        greet(sp=sp_of(wrap(me_a + step), me_b))
    greet(sp=sp_of(me_a, wrap(me_b + 1)))
    greet(sp=sp_of(me_a, wrap(me_b - 1)))
    for step in range(1, FS):
        greet(fs=fs_of(step))
    greet(tp=partner)

    greet(sp=(sp + 1) % (RING * RING))
    greet(sp=(sp + RING * RING - 1) % (RING * RING))

    lane32 = lax.broadcasted_iota(jnp.int32, (32, 128), 1)
    mine = pl.multiple_of(sp * 32, 32)
    cols = pl.ds(pl.multiple_of(f * 128, 128), 128)
    upper = f // 2
    wk = wk_ref[...].astype(F32)
    wv = wv_ref[...].astype(F32)
    pick = (lane32 * 0 + upper) > 0
    wk = jnp.where(pick, pltpu.roll(wk, 64, 1), wk)
    wv = jnp.where(pick, wv, pltpu.roll(wv, 64, 1))
    win[pl.ds(mine, 32), 0:128] = wq_ref[:, cols]
    win[pl.ds(mine, 32), 128:256] = jnp.where(lane32 < 64, wk, wv).astype(BF16)
    win[pl.ds(mine, 32), 256:384] = wc_ref[:, cols]
    win[pl.ds(mine, 32), 384:512] = wg_ref[:, cols]

    def norm_rows(start):
        def body(i, carry):
            rows = pl.ds(pl.multiple_of(start + i * 16, 16), 16)
            x = tokens_ref[rows, :].astype(F32)
            scale = lax.rsqrt(jnp.mean(x * x, axis=-1, keepdims=True) + EPSILON)
            tok[f, rows, :] = (x * scale * gain_ref[...]).astype(BF16)
            return carry

        lax.fori_loop(0, HALF // 16, body, 0)

    norm_rows(pl.multiple_of(c * HALF, HALF))

    pl.semaphore_wait(barrier, RING - 1 + 2 + FS - 1 + 1 + 2)

    def tok_rows(half, piece):
        return pl.ds(pl.multiple_of(half * HALF + piece * 64, 64), 64)

    def tok_copy(slot, half, piece, send, **where):
        ref = tok.at[slot, tok_rows(half, piece)]
        return pltpu.make_async_remote_copy(
            src_ref=ref,
            dst_ref=ref,
            send_sem=send,
            recv_sem=tok_recv.at[slot, half, piece],
            device_id=where,
            device_id_type=MESH,
        )

    def tok_first(direction, piece):
        return tok_copy(f, c, piece, tok_send.at[direction, piece], fs=fs_of(1 + 2 * direction))

    def tok_second(direction):
        slot = fs_of(3 - 2 * direction)
        return tok_copy(slot, c, direction, tok_fwd.at[direction], fs=fs_of(1 + 2 * direction))

    def tok_to_pair(slot, piece):
        return tok_copy(slot, c, piece, tok_pair.at[slot, piece], tp=partner)

    for first in range(2):
        for direction in range(2):
            tok_first(direction, (first + direction) % 2).start()

    def slab(buf, index):
        return buf.at[pl.ds(pl.multiple_of(index * 32, 32), 32)]

    def slab_copy(buf, recv, send, index, target):
        ref = slab(buf, index)
        return pltpu.make_async_remote_copy(
            src_ref=ref,
            dst_ref=ref,
            send_sem=send,
            recv_sem=recv.at[index],
            device_id={"sp": target},
            device_id_type=MESH,
        )

    def a_copy(gather, step):
        buf, recv, send_a, _ = gather
        return slab_copy(buf, recv, send_a.at[step], sp, sp_of(wrap(me_a + step), me_b))

    def b_copy(gather, direction, index):
        buf, recv, _, send_b = gather
        target = sp_of(me_a, wrap(me_b + 1 - 2 * direction))
        return slab_copy(buf, recv, send_b.at[direction, index], index, target)

    def near(j):
        odd = j % 2
        dist = (j + 1) // 2
        return wrap(me_a + odd * dist - (1 - odd) * dist)

    def start_gather(gather):
        b_copy(gather, 0, sp).start()
        b_copy(gather, 1, sp).start()

        def body(step, carry):
            a_copy(gather, step).start()
            return carry

        lax.fori_loop(1, RING, body, 0)

    def serve(gather, first, last):
        def body(n, carry):
            s, j = n // RING, n % RING
            a = near(j)

            @pl.when((s == 0) & (j > 0))
            def _():
                index = sp_of(a, me_b)
                b_copy(gather, 0, index).wait_recv()
                b_copy(gather, 0, index).start()
                b_copy(gather, 1, index).start()

            @pl.when((s > 0) & (s < 4))
            def _():
                index = sp_of(a, wrap(me_b - s))
                b_copy(gather, 0, index).wait_recv()

                @pl.when((s < 3) | (j < 4))
                def _():
                    b_copy(gather, 0, index).start()

                index = sp_of(a, wrap(me_b + s))
                b_copy(gather, 1, index).wait_recv()

                @pl.when((s < 3) | (j >= 4))
                def _():
                    b_copy(gather, 1, index).start()

            @pl.when(s == 4)
            def _():
                b_copy(gather, 0, sp_of(a, wrap(me_b + s))).wait_recv()

            return carry

        lax.fori_loop(first, last, body, 0)

    def end_gather(gather):
        def body(step, carry):
            a_copy(gather, step).wait_send()
            return carry

        lax.fori_loop(1, RING, body, 0)

        def body_b(n, carry):
            s, j = n // RING, n % RING
            a = near(j)

            @pl.when((s < 3) | (j < 4))
            def _():
                b_copy(gather, 0, sp_of(a, wrap(me_b - s))).wait_send()

            @pl.when((s < 3) | (j >= 4))
            def _():
                b_copy(gather, 1, sp_of(a, wrap(me_b + s))).wait_send()

            return carry

        lax.fori_loop(0, 4 * RING, body_b, 0)

    gather_in = (win, in_recv, in_send_a, in_send_b)
    gather_out = (wout, out_recv, out_send_a, out_send_b)
    start_gather(gather_in)

    norm_rows(pl.multiple_of(partner * HALF, HALF))
    serve(gather_in, 1, 8)

    eye = (
        lax.broadcasted_iota(jnp.int32, (32, 32), 0) == lax.broadcasted_iota(jnp.int32, (32, 32), 1)
    ).astype(BF16)
    for k in range(FS):
        rows = pl.ds(pl.multiple_of(c * 512 + k * 128, 128), 128)
        for part_at, ref in ((0, wao_ref), (128, wco_ref)):
            turned = lax.dot_general(eye, ref[rows, :], NT, preferred_element_type=F32)
            at = k * 256 + part_at
            wout[pl.ds(mine, 32), at : at + 128] = turned.astype(BF16)

    serve(gather_in, 8, 16)

    lane = lax.broadcasted_iota(jnp.int32, (HALF, 128), 1)
    frequency = jnp.exp((lane % 16).astype(F32) * (-math.log(ROPE_BASE) / 16))
    for k in range(2):
        token = lax.broadcasted_iota(jnp.int32, (HALF, 128), 0) + k * HALF
        place = jnp.where(lane % 64 < 32, sp * 4 + token // 64, token % 64)
        angle = place.astype(F32) * frequency
        ctab[k * HALF : (k + 1) * HALF, :] = jnp.cos(angle)
        sine = jnp.sin(angle)
        stab[k * HALF : (k + 1) * HALF, :] = jnp.where(lane % 32 < 16, -sine, sine)

    @pl.when(sp == 0)
    def _():
        low[...] = jnp.zeros_like(low)

    @pl.when(sp == RING * RING - 1)
    def _():
        high[...] = jnp.zeros_like(high)

    serve(gather_in, 16, 24)

    for direction in range(2):
        slot = fs_of(3 - 2 * direction)
        tok_to_pair(slot, direction).wait_recv()
        tok_second(direction).start()
        tok_to_pair(slot, direction).start()

    serve(gather_in, 24, 32)

    for direction in range(2):
        slot = fs_of(3 - 2 * direction)
        tok_to_pair(slot, 1 - direction).wait_recv()
        tok_to_pair(slot, 1 - direction).start()

    start_gather(gather_out)
    serve(gather_in, 32, 40)

    def halo_copy(i, side):
        at = side * 144
        return pltpu.make_async_remote_copy(
            src_ref=kvg.at[i, at : at + 144],
            dst_ref=(low if side else high).at[i],
            send_sem=halo_send.at[i, side],
            recv_sem=halo_recv.at[i, side],
            device_id={"sp": sp + 2 * side - 1},
            device_id_type=MESH,
        )

    lanes = lax.broadcasted_iota(jnp.int32, (TOK, 128), 1)

    def rotated(x, cosine, sine):
        other = jnp.where(lanes % 32 < 16, pltpu.roll(x, 112, 1), pltpu.roll(x, 16, 1))
        return x * cosine + other * sine

    def project(i):
        slot = fs_of(i)
        acc = jnp.dot(tok[slot], win[...], preferred_element_type=F32)
        cosine, sine = ctab[...], stab[...]
        query = rotated(acc[:, 0:128], cosine, sine).astype(BF16).astype(F32) * HEAD_DIM**-0.5
        qbuf[i, 0] = jnp.where(lanes < 64, query, 0.0).astype(BF16)
        qbuf[i, 1] = jnp.where(lanes < 64, pltpu.roll(query, 64, 1), 0.0).astype(BF16)
        pair = acc[:, 128:256]
        turned = rotated(pair, cosine, sine)
        kvg[i, 16:272] = jnp.where(lanes < 64, turned, pair).astype(BF16)
        glu = (acc[:, 256:384] * jax.nn.sigmoid(acc[:, 384:512])).astype(BF16)
        kvg[i, 0:16] = glu[0:16]
        kvg[i, 272:288] = glu[240:256]
        gext[i, 16:272] = glu.astype(F32)

        @pl.when(has_low)
        def _():
            halo_copy(i, 0).start()

        @pl.when(has_high)
        def _():
            halo_copy(i, 1).start()

    row_at = lax.broadcasted_iota(jnp.int32, (HALF, 256), 0)
    key_at = lax.broadcasted_iota(jnp.int32, (HALF, 256), 1)
    half_row = lax.broadcasted_iota(jnp.int32, (HALF, 128), 0)
    half_key = lax.broadcasted_iota(jnp.int32, (HALF, 128), 1)
    half_lane = half_key
    far = RING * TOK
    own_valid = (key_at - row_at <= WINDOW, key_at >= row_at)
    halo_valid = (
        half_key >= half_row + jnp.where(has_low, 0, far),
        half_key + jnp.where(has_high, 0, far) <= half_row,
    )

    def mix(i):
        @pl.when(has_low)
        def _():
            halo_copy(i, 1).wait_recv()

        @pl.when(has_high)
        def _():
            halo_copy(i, 0).wait_recv()

        own_kv = kvg[i, 16:272]
        own_ones = jnp.where(
            lax.broadcasted_iota(jnp.int32, (TOK, 128), 1) < 64, jnp.ones_like(own_kv), own_kv
        )
        for block in range(2):
            near_kv = low[i, 0:128] if block == 0 else high[i, 16:144]
            near_ones = jnp.where(half_lane < 64, jnp.ones_like(near_kv), near_kv)
            heads = []
            for h in range(2):
                q = qbuf[i, h, block * HALF : (block + 1) * HALF]
                s_own = lax.dot_general(q, own_kv, NT, preferred_element_type=F32)
                s_near = lax.dot_general(q, near_kv, NT, preferred_element_type=F32)
                s_own = jnp.where(own_valid[block], s_own, NEGATIVE)
                s_near = jnp.where(halo_valid[block], s_near, NEGATIVE)
                sink = sink_ref[2 * f + h]
                top = jnp.maximum(
                    jnp.maximum(s_own[:, 0:128], s_own[:, 128:256]), s_near
                )
                top = jnp.maximum(jnp.max(top, axis=-1, keepdims=True), sink)
                p_own = jnp.exp(s_own - top).astype(BF16)
                p_near = jnp.exp(s_near - top).astype(BF16)
                mixed = jnp.dot(p_own, own_ones, preferred_element_type=F32) + jnp.dot(
                    p_near, near_ones, preferred_element_type=F32
                )
                heads.append(mixed / (pltpu.roll(mixed, 64, 1) + jnp.exp(sink - top)))
            joined = jnp.where(half_lane < 64, pltpu.roll(heads[0], 64, 1), heads[1])
            sbuf[i, block * HALF : (block + 1) * HALF, 0:128] = joined.astype(BF16)

        gext[i, 0:16] = low[i, 128:144].astype(F32)
        gext[i, 272:288] = high[i, 0:16].astype(F32)

        for block in range(4):
            total = jnp.zeros((64, 128), F32)
            for k in range(TAPS):
                at = block * 64 + k + 1
                total = total + taps_ref[k : k + 1, cols] * gext[i, at : at + 64]
            sbuf[i, block * 64 : (block + 1) * 64, 128:256] = total.astype(BF16)

    def feat_copy(i):
        return pltpu.make_async_remote_copy(
            src_ref=sbuf.at[i],
            dst_ref=feat.at[f],
            send_sem=feat_send.at[i],
            recv_sem=feat_recv.at[f],
            device_id={"fs": fs_of(i)},
            device_id_type=MESH,
        )

    def wait_pair(slot):
        tok_copy(slot, partner, 0, tok_fwd.at[0], tp=partner).wait_recv()
        tok_copy(slot, partner, 1, tok_fwd.at[0], tp=partner).wait_recv()

    project(0)
    serve(gather_out, 1, 8)
    wait_pair(fs_of(1))
    project(1)
    wait_pair(fs_of(3))
    project(3)
    serve(gather_out, 8, 12)
    mix(0)
    feat[f] = sbuf[0]
    for piece in range(2):
        tok_to_pair(fs_of(2), piece).wait_recv()
        tok_to_pair(fs_of(2), piece).start()
    serve(gather_out, 12, 16)
    wait_pair(fs_of(2))
    project(2)
    mix(1)
    feat_copy(1).start()
    serve(gather_out, 16, 20)
    mix(3)
    feat_copy(3).start()
    serve(gather_out, 20, 24)
    mix(2)
    feat_copy(2).start()
    serve(gather_out, 24, 32)

    def feat_wait(src):
        pltpu.make_async_remote_copy(
            src_ref=sbuf.at[0],
            dst_ref=feat.at[src],
            send_sem=feat_send.at[0],
            recv_sem=feat_recv.at[src],
            device_id={"tp": partner},
            device_id_type=MESH,
        ).wait_recv()

    for i in (1, 3, 2):
        feat_wait(fs_of(i))

    total = jnp.zeros((TOK, 1), F32)
    for k in range(FS):
        values = feat[k, :, 128:256].astype(F32) + bias_ref[:, k * 128 : (k + 1) * 128]
        cvals[:, k * 128 : (k + 1) * 128] = values
        total = total + jnp.sum(values, axis=-1, keepdims=True)
    here = total / 512.0
    around = jnp.zeros((TOK, 1), F32)
    for k in range(FS):
        centred = cvals[:, k * 128 : (k + 1) * 128] - here
        around = around + jnp.sum(centred * centred, axis=-1, keepdims=True)
    stat_out[...] = jnp.where(lanes < 64, here, around)
    stat_copy = pltpu.make_async_remote_copy(
        src_ref=stat_out,
        dst_ref=stat_in,
        send_sem=stat_sem.at[0],
        recv_sem=stat_sem.at[1],
        device_id={"tp": partner},
        device_id_type=MESH,
    )
    stat_copy.start()
    for k in range(FS):
        raw[:, k * 256 : k * 256 + 128] = feat[k, :, 0:128]
    stat_copy.wait_recv()
    there = stat_in[:, 0:1]
    gap = here - there
    centre = 0.5 * (here + there)
    spread = (around + stat_in[:, 64:65] + 256.0 * gap * gap) / 1024.0
    scale = lax.rsqrt(spread + EPSILON)
    for k in range(FS):
        at = slice(k * 128, (k + 1) * 128)
        v = (cvals[:, at] - centre) * scale * cgain_ref[:, at] + cshift_ref[:, at]
        raw[:, k * 256 + 128 : (k + 1) * 256] = (v / (1.0 + jnp.exp(-v))).astype(BF16)

    serve(gather_out, 32, 40)

    def part_copy(n):
        return pltpu.make_async_remote_copy(
            src_ref=part_out.at[n],
            dst_ref=part_in.at[n],
            send_sem=part_send.at[n],
            recv_sem=part_recv.at[n],
            device_id={"tp": partner},
            device_id_type=MESH,
        )

    mine_rows = pl.ds(pl.multiple_of(c * HALF, HALF), HALF)
    other_rows = pl.ds(pl.multiple_of(partner * HALF, HALF), HALF)
    for n in range(D // CHUNK):
        weights = wout[n * CHUNK : (n + 1) * CHUNK, :]
        part_out[n] = lax.dot_general(
            raw[other_rows, :], weights, NT, preferred_element_type=F32
        ).astype(BF16)
        part_copy(n).start()
        part[n] = lax.dot_general(raw[mine_rows, :], weights, NT, preferred_element_type=F32)
    for n in range(D // CHUNK):
        part_copy(n).wait_recv()
        out_ref[:, n * CHUNK : (n + 1) * CHUNK] = (part[n] + part_in[n].astype(F32)).astype(BF16)

    for n in range(D // CHUNK):
        part_copy(n).wait_send()
    stat_copy.wait_send()
    for i in range(1, FS):
        feat_copy(i).wait_send()
    for i in range(FS):

        @pl.when(has_low)
        def _():
            halo_copy(i, 0).wait_send()

        @pl.when(has_high)
        def _():
            halo_copy(i, 1).wait_send()

    for direction in range(2):
        for piece in range(2):
            tok_first(direction, piece).wait_send()
        tok_second(direction).wait_send()
    for i in range(1, FS):
        for piece in range(2):
            tok_to_pair(fs_of(i), piece).wait_send()
    end_gather(gather_in)
    end_gather(gather_out)


def local(
    tokens,
    norm_gain,
    w_query,
    w_key,
    w_value,
    w_conv_in,
    w_conv_gate,
    sink_logit,
    conv_taps,
    conv_bias,
    channel_gain,
    channel_shift,
    w_attn_out,
    w_conv_out,
):
    vmem = pl.BlockSpec(memory_space=pltpu.VMEM)
    smem = pl.BlockSpec(memory_space=pltpu.SMEM)
    dma = pltpu.SemaphoreType.DMA
    return pl.pallas_call(
        kernel,
        out_shape=jax.ShapeDtypeStruct((HALF, D), BF16),
        in_specs=[vmem] * 7 + [smem] + [vmem] * 6,
        out_specs=vmem,
        scratch_shapes=[
            pltpu.VMEM((FS, TOK, D), BF16),
            pltpu.VMEM((D, 512), BF16),
            pltpu.VMEM((D, 1024), BF16),
            pltpu.VMEM((TOK, 128), F32),
            pltpu.VMEM((TOK, 128), F32),
            pltpu.VMEM((FS, 2, TOK, 128), BF16),
            pltpu.VMEM((FS, 288, 128), BF16),
            pltpu.VMEM((FS, 288, 128), F32),
            pltpu.VMEM((FS, 144, 128), BF16),
            pltpu.VMEM((FS, 144, 128), BF16),
            pltpu.VMEM((FS, TOK, 256), BF16),
            pltpu.VMEM((FS, TOK, 256), BF16),
            pltpu.VMEM((TOK, 1024), BF16),
            pltpu.VMEM((TOK, 512), F32),
            pltpu.VMEM((TOK, 128), F32),
            pltpu.VMEM((TOK, 128), F32),
            pltpu.VMEM((D // CHUNK, HALF, CHUNK), F32),
            pltpu.VMEM((D // CHUNK, HALF, CHUNK), BF16),
            pltpu.VMEM((D // CHUNK, HALF, CHUNK), BF16),
            dma((64,)),
            dma((RING,)),
            dma((2, 64)),
            dma((64,)),
            dma((RING,)),
            dma((2, 64)),
            dma((FS, 2, 2)),
            dma((2, 2)),
            dma((2,)),
            dma((FS, 2)),
            dma((FS, 2)),
            dma((FS, 2)),
            dma((FS,)),
            dma((FS,)),
            dma((2,)),
            dma((D // CHUNK,)),
            dma((D // CHUNK,)),
        ],
        compiler_params=pltpu.CompilerParams(
            collective_id=0, has_side_effects=True, vmem_limit_bytes=60 * 1024 * 1024
        ),
        name="fused",
    )(
        tokens,
        norm_gain.reshape(1, -1),
        w_query,
        w_key,
        w_value,
        w_conv_in,
        w_conv_gate,
        sink_logit,
        conv_taps,
        conv_bias.reshape(1, -1),
        channel_gain.reshape(1, -1),
        channel_shift.reshape(1, -1),
        w_attn_out,
        w_conv_out,
    )


def solution(mesh):
    in_specs = (
        P(("fs", "sp"), None),
        P(),
        P("sp", "tp"),
        P("sp", "tp"),
        P("sp", "tp"),
        P("sp", "tp"),
        P("sp", "tp"),
        P("tp"),
        P(None, "tp"),
        P("tp"),
        P("tp"),
        P("tp"),
        P(None, "sp"),
        P(None, "sp"),
    )
    out_specs = P(("fs", "sp", "tp"), None)
    return jax.shard_map(local, mesh=mesh, in_specs=in_specs, out_specs=out_specs, check_vma=False)
```

time: 216 us -> 88.1 us (0.41)
  waiting for transfers between devices: 146 us -> 0 us
  Pallas kernels: 0 us -> 83.4 us
  blocking collectives: 15.1 us -> 0 us
  matrix products: 13.8 us -> 0 us
  between operations: 13.7 us -> 0.01 us
  starting transfers between devices: 9.34 us -> 0 us
  other arithmetic: 8.51 us -> 0 us
  local copies, waits for them, and re-layouts: 8.34 us -> 4.43 us
    all_gather x2 -> x0, waiting for transfers between devices: 146 us -> none  [the longest x1 93.4 us: in_one_piece(): result = lax.all_gather(both, axis, axis=dim, tiled=True)]
    pallas_call x0 -> x1, Pallas kernels: none -> 83.4 us  [local(): pl.pallas_call(kernel, out_shape=jax.ShapeDtypeStruct((HALF, D), BF16), i...]
    dot_general x6 -> x0, matrix products: 13.8 us -> none  [the longest x1 3.48 us: local(): jnp.dot(normed, jnp.concatenate([piece_conv, piece_gate], axis=1), prefer...]
    ppermute x4 -> x0, starting transfers between devices: 9.3 us -> none  [the longest x2 6.71 us: padded(): lax.ppermute(lax.slice_in_dim(block, block.shape[dim] - width, None, axis...]
    all_to_all x1 -> x0, blocking collectives: 9.02 us -> none  [sum_at_owner(): parts = lax.all_to_all(cut_along(array, dim, count), axis, 0, 0, tiled=True)]
    reduce_sum x6 -> x0, other arithmetic: 6.62 us -> none  [the longest x1 3.07 us: local(): jnp.sum(filtered, axis=-1)]
    all_gather x2 -> x0, blocking collectives: 6.08 us -> none  [over_pieces(): return lax.all_gather(array, axis).sum(0)]
    slice x6 -> x0, local copies, waits for them, and re-layouts: 2.23 us -> none  [the longest x2 2.18 us: local(): conv_taps[shift_index][None, :]]
  transfers between devices with their start and end apart: 6 -> 0, of which waited for: 3 -> 0; matrix products, arithmetic and copies ran while one was open for 10% -> 0% of each run, Pallas kernels for 0% -> 0%
where the time goes in v1:
time: 88.1 us; the launch traced here: 87.9 us
  Pallas kernels  83.4 us (95%)
  local copies, waits for them, and re-layouts  4.43 us (5%)
    pallas_call x1, Pallas kernels, local(): pl.pallas_call(kernel, out_shape=jax.ShapeDtypeStruct((HALF, D), BF16), i...  83.4 us
    unnamed x5, local copies, waits for them, and re-layouts  4.43 us

profile of v1, /device:TPU:1, one launch (start us, length us, event | category | flops | bytes accessed | tf_op | source)
XLA Modules:
  0.0 87.9 jit_solution(12025458619199508879)
XLA Ops:
  0.0 0.0 copy-start
  0.0 1.7 %copy.15.wao_ref = bf16[1024,32]{1,0:T(8,128)(2,1)} copy(bf16[1024,32]{0,1:T(8,128)(2,1)} %param.26) | data formatting | bytes 131072 | tf_op args[12]
  1.7 0.0 copy-done
  1.7 0.8 copy.16.wco_ref
  2.5 83.4 %fused.1 = bf16[128,2048]{1,0:T(8,128)(2,1)} custom-call(bf16[256,2048]{1,0:T(8,128)(2,1)} %tokens_ref.1, f32[1,2048]{1,0:T(1,128)} %bitcast.4, bf16[32,512]{1,0:T(8,128)(2,1)} %wq_ref.1, bf16[32,128]{1,0:T(8,128)(2,1)} %wk_ref.1, bf16[32,128]{1,0:T(8,128)(2,1)} %wv_ref.1, bf16[32,512]{1,0:T(8,128)(2,1)} %wc_ref.1, bf16[32,512]{1,0:T(8,128)(2,1)} %wg_ref.1, ...), custom_call_target="tpu_custom_call" | custom-call | tf_op jit(solution)/shard_map/fused/pallas_call | solution.py:580
  86.0 1.9 %copy.18 = bf16[128,2048]{1,0:T(8,128)(2,1)} copy(bf16[128,2048]{1,0:T(8,128)(2,1)} %fused.1) | data formatting | bytes 1048576
Async XLA Ops:
  0.0 1.7 %copy-start = (bf16[1024,32]{0,1:T(8,128)(2,1)S(1)}, bf16[1024,32]{0,1:T(8,128)(2,1)}, u32[]{:S(2)}) copy-start(bf16[1024,32]{0,1:T(8,128)(2,1)} %param.27) | copy-start | bytes 196612

commit v2 on v1

--- a/solution.py
+++ b/solution.py
@@ -26,59 +26,72 @@
 BF16 = jnp.bfloat16
 
 
-def kernel(
-    tokens_ref,
-    gain_ref,
-    wq_ref,
-    wk_ref,
-    wv_ref,
-    wc_ref,
-    wg_ref,
-    sink_ref,
-    taps_ref,
-    bias_ref,
-    cgain_ref,
-    cshift_ref,
-    wao_ref,
-    wco_ref,
-    out_ref,
-    tok,
-    win,
-    wout,
-    ctab,
-    stab,
-    qbuf,
-    kvg,
-    gext,
-    low,
-    high,
-    sbuf,
-    feat,
-    raw,
-    cvals,
-    stat_out,
-    stat_in,
-    part,
-    part_out,
-    part_in,
-    in_recv,
-    in_send_a,
-    in_send_b,
-    out_recv,
-    out_send_a,
-    out_send_b,
-    tok_recv,
-    tok_send,
-    tok_fwd,
-    tok_pair,
-    halo_recv,
-    halo_send,
-    feat_recv,
-    feat_send,
-    stat_sem,
-    part_recv,
-    part_send,
-):
+def kernel(*refs):
+    (
+        tokens_hbm,
+        gain_hbm,
+        wq_hbm,
+        wk_hbm,
+        wv_hbm,
+        wc_hbm,
+        wg_hbm,
+        sink_hbm,
+        taps_hbm,
+        bias_hbm,
+        cgain_hbm,
+        cshift_hbm,
+        wao_hbm,
+        wco_hbm,
+        out_ref,
+        tokens_ref,
+        gain_ref,
+        wq_ref,
+        wk_ref,
+        wv_ref,
+        wc_ref,
+        wg_ref,
+        sink_ref,
+        taps_ref,
+        bias_ref,
+        cgain_ref,
+        cshift_ref,
+        wao_ref,
+        wco_ref,
+        tok,
+        win,
+        wout,
+        ctab,
+        stab,
+        qbuf,
+        kvg,
+        gext,
+        low,
+        high,
+        sbuf,
+        feat,
+        raw,
+        cvals,
+        stat_out,
+        stat_in,
+        part,
+        part_out,
+        part_in,
+        load_sem,
+        in_recv_a,
+        in_recv_b,
+        out_recv_a,
+        out_recv_b,
+        tok_recv,
+        halo_recv,
+        feat_recv,
+        stat_recv,
+        part_recv,
+        send_sem,
+    ) = refs
+    in_sent, out_sent, tok_sent, feat_sent, stat_sent, part_sent = (
+        send_sem.at[k] for k in range(6)
+    )
+    halo_sent = (send_sem.at[6], send_sem.at[7])
     sp = lax.axis_index("sp")
     f = lax.axis_index("fs")
     c = lax.axis_index("tp")
@@ -96,6 +109,34 @@
     def fs_of(step):
         return (f + step) % FS
 
+    def load(k, src, dst):
+        copy = pltpu.make_async_copy(src, dst, load_sem.at[k])
+        copy.start()
+        return copy
+
+    own_half = pl.ds(pl.multiple_of(c * HALF, HALF), HALF)
+    other_half = pl.ds(pl.multiple_of(partner * HALF, HALF), HALF)
+    load_weights = [
+        load(0, wq_hbm, wq_ref),
+        load(1, wk_hbm, wk_ref),
+        load(2, wv_hbm, wv_ref),
+        load(3, wc_hbm, wc_ref),
+        load(4, wg_hbm, wg_ref),
+    ]
+    load_own = [
+        load(5, gain_hbm, gain_ref),
+        load(6, tokens_hbm.at[own_half], tokens_ref.at[own_half]),
+    ]
+    load_other = load(7, tokens_hbm.at[other_half], tokens_ref.at[other_half])
+    load_out = [load(8, wao_hbm, wao_ref), load(9, wco_hbm, wco_ref)]
+    load_rest = [
+        load(10, sink_hbm, sink_ref),
+        load(11, taps_hbm, taps_ref),
+        load(12, bias_hbm, bias_ref),
+        load(13, cgain_hbm, cgain_ref),
+        load(14, cshift_hbm, cshift_ref),
+    ]
+
     has_low = sp > 0
     has_high = sp < RING * RING - 1
 
@@ -119,6 +160,8 @@
     mine = pl.multiple_of(sp * 32, 32)
     cols = pl.ds(pl.multiple_of(f * 128, 128), 128)
     upper = f // 2
+    for copy in load_weights:
+        copy.wait()
     wk = wk_ref[...].astype(F32)
     wv = wv_ref[...].astype(F32)
     pick = (lane32 * 0 + upper) > 0
@@ -139,6 +182,8 @@
 
         lax.fori_loop(0, HALF // 16, body, 0)
 
+    for copy in load_own:
+        copy.wait()
     norm_rows(pl.multiple_of(c * HALF, HALF))
 
     pl.semaphore_wait(barrier, RING - 1 + 2 + FS - 1 + 1 + 2)
@@ -146,26 +191,26 @@
     def tok_rows(half, piece):
         return pl.ds(pl.multiple_of(half * HALF + piece * 64, 64), 64)
 
-    def tok_copy(slot, half, piece, send, **where):
+    def tok_copy(slot, half, piece, **where):
         ref = tok.at[slot, tok_rows(half, piece)]
         return pltpu.make_async_remote_copy(
             src_ref=ref,
             dst_ref=ref,
-            send_sem=send,
+            send_sem=tok_sent,
             recv_sem=tok_recv.at[slot, half, piece],
             device_id=where,
             device_id_type=MESH,
         )
 
     def tok_first(direction, piece):
-        return tok_copy(f, c, piece, tok_send.at[direction, piece], fs=fs_of(1 + 2 * direction))
+        return tok_copy(f, c, piece, fs=fs_of(1 + 2 * direction))
 
     def tok_second(direction):
         slot = fs_of(3 - 2 * direction)
-        return tok_copy(slot, c, direction, tok_fwd.at[direction], fs=fs_of(1 + 2 * direction))
+        return tok_copy(slot, c, direction, fs=fs_of(1 + 2 * direction))
 
     def tok_to_pair(slot, piece):
-        return tok_copy(slot, c, piece, tok_pair.at[slot, piece], tp=partner)
+        return tok_copy(slot, c, piece, tp=partner)
 
     for first in range(2):
         for direction in range(2):
@@ -174,118 +219,128 @@
     def slab(buf, index):
         return buf.at[pl.ds(pl.multiple_of(index * 32, 32), 32)]
 
-    def slab_copy(buf, recv, send, index, target):
+    def slab_copy(buf, recv, sent, index, target):
         ref = slab(buf, index)
         return pltpu.make_async_remote_copy(
             src_ref=ref,
             dst_ref=ref,
-            send_sem=send,
-            recv_sem=recv.at[index],
+            send_sem=sent,
+            recv_sem=recv,
             device_id={"sp": target},
             device_id_type=MESH,
         )
 
-    def a_copy(gather, step):
-        buf, recv, send_a, _ = gather
-        return slab_copy(buf, recv, send_a.at[step], sp, sp_of(wrap(me_a + step), me_b))
-
-    def b_copy(gather, direction, index):
-        buf, recv, _, send_b = gather
+    def a_copy(gather, a, step):
+        buf, recv_a, _, sent = gather
+        target = sp_of(wrap(me_a + step), me_b)
+        return slab_copy(buf, recv_a.at[a], sent, sp_of(a, me_b), target)
+
+    def b_copy(gather, direction, j, b):
+        buf, _, recv_b, sent = gather
         target = sp_of(me_a, wrap(me_b + 1 - 2 * direction))
-        return slab_copy(buf, recv, send_b.at[direction, index], index, target)
+        return slab_copy(buf, recv_b.at[b, j // 2], sent, sp_of(near(j), b), target)
+
+    def wait_pair_of_slabs(gather, pair, b):
+        buf, _, recv_b, sent = gather
+        ref = buf.at[0:64]
+        pltpu.make_async_remote_copy(
+            src_ref=ref,
+            dst_ref=ref,
+            send_sem=sent,
+            recv_sem=recv_b.at[b, pair],
+            device_id={"tp": partner},
+            device_id_type=MESH,
+        ).wait_recv()
 
     def near(j):
         odd = j % 2
         dist = (j + 1) // 2
         return wrap(me_a + odd * dist - (1 - odd) * dist)
 
-    def start_gather(gather):
-        b_copy(gather, 0, sp).start()
-        b_copy(gather, 1, sp).start()
+    def start_gather(gather, relay):
+        b_copy(gather, 0, 0, me_b).start()
+        b_copy(gather, 1, 0, me_b).start()
 
         def body(step, carry):
-            a_copy(gather, step).start()
+            a_copy(gather, me_a, step).start()
             return carry
 
-        lax.fori_loop(1, RING, body, 0)
-
-    def serve(gather, first, last):
-        def body(n, carry):
-            s, j = n // RING, n % RING
+        if relay:
+            a_copy(gather, me_a, 1).start()
+            a_copy(gather, me_a, -1).start()
+        else:
+            lax.fori_loop(1, RING, body, 0)
+
+    def serve_a(gather, first, last, relay):
+        def body(j, carry):
             a = near(j)
-
-            @pl.when((s == 0) & (j > 0))
-            def _():
-                index = sp_of(a, me_b)
-                b_copy(gather, 0, index).wait_recv()
-                b_copy(gather, 0, index).start()
-                b_copy(gather, 1, index).start()
-
-            @pl.when((s > 0) & (s < 4))
-            def _():
-                index = sp_of(a, wrap(me_b - s))
-                b_copy(gather, 0, index).wait_recv()
-
-                @pl.when((s < 3) | (j < 4))
+            a_copy(gather, a, 1).wait_recv()
+            b_copy(gather, 0, j, me_b).start()
+            b_copy(gather, 1, j, me_b).start()
+            if relay:
+
+                @pl.when(j % 2 == 0)
                 def _():
-                    b_copy(gather, 0, index).start()
-
-                index = sp_of(a, wrap(me_b + s))
-                b_copy(gather, 1, index).wait_recv()
-
-                @pl.when((s < 3) | (j >= 4))
+                    a_copy(gather, a, 1).start()
+
+                @pl.when((j % 2 == 1) & (j < 5))
                 def _():
-                    b_copy(gather, 1, index).start()
-
-            @pl.when(s == 4)
-            def _():
-                b_copy(gather, 0, sp_of(a, wrap(me_b + s))).wait_recv()
+                    a_copy(gather, a, -1).start()
 
             return carry
 
         lax.fori_loop(first, last, body, 0)
 
+    def serve_b(gather, step, first, last):
+        def body(pair, carry):
+            for direction in range(2):
+                b = wrap(me_b - step if direction == 0 else me_b + step)
+                wait_pair_of_slabs(gather, pair, b)
+
+                def forward(b=b, direction=direction):
+                    b_copy(gather, direction, 2 * pair, b).start()
+                    b_copy(gather, direction, 2 * pair + 1, b).start()
+
+                if step < 3:
+                    forward()
+                else:
+                    pl.when(pair < 2 if direction == 0 else pair >= 2)(forward)
+            return carry
+
+        def body_last(pair, carry):
+            wait_pair_of_slabs(gather, pair, wrap(me_b + step))
+            return carry
+
+        lax.fori_loop(first, last, body if step < 4 else body_last, 0)
+
     def end_gather(gather):
-        def body(step, carry):
-            a_copy(gather, step).wait_send()
-            return carry
-
-        lax.fori_loop(1, RING, body, 0)
-
-        def body_b(n, carry):
-            s, j = n // RING, n % RING
-            a = near(j)
-
-            @pl.when((s < 3) | (j < 4))
-            def _():
-                b_copy(gather, 0, sp_of(a, wrap(me_b - s))).wait_send()
-
-            @pl.when((s < 3) | (j >= 4))
-            def _():
-                b_copy(gather, 1, sp_of(a, wrap(me_b + s))).wait_send()
-
-            return carry
-
-        lax.fori_loop(0, 4 * RING, body_b, 0)
-
-    gather_in = (win, in_recv, in_send_a, in_send_b)
-    gather_out = (wout, out_recv, out_send_a, out_send_b)
-    start_gather(gather_in)
-
+        buf, _, _, sent = gather
+        ref = buf.at[0 : 63 * 32]
+        pltpu.make_async_remote_copy(
+            src_ref=ref,
+            dst_ref=ref,
+            send_sem=sent,
+            recv_sem=stat_recv.at[0],
+            device_id={"tp": partner},
+            device_id_type=MESH,
+        ).wait_send()
+
+    gather_in = (win, in_recv_a, in_recv_b, in_sent)
+    gather_out = (wout, out_recv_a, out_recv_b, out_sent)
+    start_gather(gather_in, False)
+
+    load_other.wait()
     norm_rows(pl.multiple_of(partner * HALF, HALF))
-    serve(gather_in, 1, 8)
-
-    eye = (
-        lax.broadcasted_iota(jnp.int32, (32, 32), 0) == lax.broadcasted_iota(jnp.int32, (32, 32), 1)
-    ).astype(BF16)
+    for copy in load_out:
+        copy.wait()
     for k in range(FS):
-        rows = pl.ds(pl.multiple_of(c * 512 + k * 128, 128), 128)
-        for part_at, ref in ((0, wao_ref), (128, wco_ref)):
-            turned = lax.dot_general(eye, ref[rows, :], NT, preferred_element_type=F32)
-            at = k * 256 + part_at
-            wout[pl.ds(mine, 32), at : at + 128] = turned.astype(BF16)
-
-    serve(gather_in, 8, 16)
+        at = pl.ds(pl.multiple_of(c * 512 + k * 128, 128), 128)
+        wout[pl.ds(mine, 32), k * 256 : k * 256 + 128] = wao_ref[:, at]
+        wout[pl.ds(mine, 32), k * 256 + 128 : (k + 1) * 256] = wco_ref[:, at]
+
+    serve_a(gather_in, 1, 8, False)
+    start_gather(gather_out, True)
+    serve_b(gather_in, 1, 0, 4)
 
     lane = lax.broadcasted_iota(jnp.int32, (HALF, 128), 1)
     frequency = jnp.exp((lane % 16).astype(F32) * (-math.log(ROPE_BASE) / 16))
@@ -305,7 +360,9 @@
     def _():
         high[...] = jnp.zeros_like(high)
 
-    serve(gather_in, 16, 24)
+    serve_a(gather_out, 1, 3, True)
+    serve_b(gather_in, 2, 0, 4)
+    serve_a(gather_out, 3, 5, True)
 
     for direction in range(2):
         slot = fs_of(3 - 2 * direction)
@@ -313,22 +370,25 @@
         tok_second(direction).start()
         tok_to_pair(slot, direction).start()
 
-    serve(gather_in, 24, 32)
+    serve_b(gather_in, 3, 0, 4)
+    serve_a(gather_out, 5, 7, True)
 
     for direction in range(2):
         slot = fs_of(3 - 2 * direction)
         tok_to_pair(slot, 1 - direction).wait_recv()
         tok_to_pair(slot, 1 - direction).start()
 
-    start_gather(gather_out)
-    serve(gather_in, 32, 40)
+    serve_b(gather_in, 4, 0, 4)
+    serve_a(gather_out, 7, 8, True)
+    for copy in load_rest:
+        copy.wait()
 
     def halo_copy(i, side):
         at = side * 144
         return pltpu.make_async_remote_copy(
             src_ref=kvg.at[i, at : at + 144],
             dst_ref=(low if side else high).at[i],
-            send_sem=halo_send.at[i, side],
+            send_sem=halo_sent[side],
             recv_sem=halo_recv.at[i, side],
             device_id={"sp": sp + 2 * side - 1},
             device_id_type=MESH,
@@ -375,6 +435,12 @@
         half_key + jnp.where(has_high, 0, far) <= half_row,
     )
 
+    head_lane = lax.broadcasted_iota(jnp.int32, (1, 8), 1)
+    sinks = [
+        jnp.sum(jnp.where(head_lane == 2 * f + h, sink_ref[...], 0.0), axis=-1, keepdims=True)
+        for h in range(2)
+    ]
+
     def mix(i):
         @pl.when(has_low)
         def _():
@@ -398,7 +464,7 @@
                 s_near = lax.dot_general(q, near_kv, NT, preferred_element_type=F32)
                 s_own = jnp.where(own_valid[block], s_own, NEGATIVE)
                 s_near = jnp.where(halo_valid[block], s_near, NEGATIVE)
-                sink = sink_ref[2 * f + h]
+                sink = sinks[h]
                 top = jnp.maximum(
                     jnp.maximum(s_own[:, 0:128], s_own[:, 128:256]), s_near
                 )
@@ -426,46 +492,49 @@
         return pltpu.make_async_remote_copy(
             src_ref=sbuf.at[i],
             dst_ref=feat.at[f],
-            send_sem=feat_send.at[i],
+            send_sem=feat_sent,
             recv_sem=feat_recv.at[f],
             device_id={"fs": fs_of(i)},
             device_id_type=MESH,
         )
 
     def wait_pair(slot):
-        tok_copy(slot, partner, 0, tok_fwd.at[0], tp=partner).wait_recv()
-        tok_copy(slot, partner, 1, tok_fwd.at[0], tp=partner).wait_recv()
+        tok_copy(slot, partner, 0, tp=partner).wait_recv()
+        tok_copy(slot, partner, 1, tp=partner).wait_recv()
 
     project(0)
-    serve(gather_out, 1, 8)
+    serve_b(gather_out, 1, 0, 1)
     wait_pair(fs_of(1))
     project(1)
+    serve_b(gather_out, 1, 1, 2)
     wait_pair(fs_of(3))
     project(3)
-    serve(gather_out, 8, 12)
-    mix(0)
-    feat[f] = sbuf[0]
     for piece in range(2):
         tok_to_pair(fs_of(2), piece).wait_recv()
         tok_to_pair(fs_of(2), piece).start()
-    serve(gather_out, 12, 16)
+    serve_b(gather_out, 1, 2, 3)
+    mix(0)
+    feat[f] = sbuf[0]
+    serve_b(gather_out, 1, 3, 4)
     wait_pair(fs_of(2))
     project(2)
+    serve_b(gather_out, 2, 0, 1)
     mix(1)
     feat_copy(1).start()
-    serve(gather_out, 16, 20)
+    serve_b(gather_out, 2, 1, 3)
     mix(3)
     feat_copy(3).start()
-    serve(gather_out, 20, 24)
+    serve_b(gather_out, 2, 3, 4)
+    serve_b(gather_out, 3, 0, 1)
     mix(2)
     feat_copy(2).start()
-    serve(gather_out, 24, 32)
+    serve_b(gather_out, 3, 1, 4)
 
     def feat_wait(src):
         pltpu.make_async_remote_copy(
             src_ref=sbuf.at[0],
             dst_ref=feat.at[src],
-            send_sem=feat_send.at[0],
+            send_sem=feat_sent,
             recv_sem=feat_recv.at[src],
             device_id={"tp": partner},
             device_id_type=MESH,
@@ -488,8 +557,8 @@
     stat_copy = pltpu.make_async_remote_copy(
         src_ref=stat_out,
         dst_ref=stat_in,
-        send_sem=stat_sem.at[0],
-        recv_sem=stat_sem.at[1],
+        send_sem=stat_sent,
+        recv_sem=stat_recv.at[0],
         device_id={"tp": partner},
         device_id_type=MESH,
     )
@@ -507,53 +576,52 @@
         v = (cvals[:, at] - centre) * scale * cgain_ref[:, at] + cshift_ref[:, at]
         raw[:, k * 256 + 128 : (k + 1) * 256] = (v / (1.0 + jnp.exp(-v))).astype(BF16)
 
-    serve(gather_out, 32, 40)
+    serve_b(gather_out, 4, 0, 4)
 
     def part_copy(n):
         return pltpu.make_async_remote_copy(
             src_ref=part_out.at[n],
             dst_ref=part_in.at[n],
-            send_sem=part_send.at[n],
+            send_sem=part_sent,
             recv_sem=part_recv.at[n],
             device_id={"tp": partner},
             device_id_type=MESH,
         )
 
-    mine_rows = pl.ds(pl.multiple_of(c * HALF, HALF), HALF)
-    other_rows = pl.ds(pl.multiple_of(partner * HALF, HALF), HALF)
     for n in range(D // CHUNK):
         weights = wout[n * CHUNK : (n + 1) * CHUNK, :]
         part_out[n] = lax.dot_general(
-            raw[other_rows, :], weights, NT, preferred_element_type=F32
+            raw[other_half, :], weights, NT, preferred_element_type=F32
         ).astype(BF16)
         part_copy(n).start()
-        part[n] = lax.dot_general(raw[mine_rows, :], weights, NT, preferred_element_type=F32)
+        part[n] = lax.dot_general(raw[own_half, :], weights, NT, preferred_element_type=F32)
     for n in range(D // CHUNK):
         part_copy(n).wait_recv()
         out_ref[:, n * CHUNK : (n + 1) * CHUNK] = (part[n] + part_in[n].astype(F32)).astype(BF16)
 
-    for n in range(D // CHUNK):
-        part_copy(n).wait_send()
+    def drain(ref, sent):
+        pltpu.make_async_remote_copy(
+            src_ref=ref,
+            dst_ref=ref,
+            send_sem=sent,
+            recv_sem=stat_recv.at[0],
+            device_id={"tp": partner},
+            device_id_type=MESH,
+        ).wait_send()
+
+    drain(part_out, part_sent)
     stat_copy.wait_send()
-    for i in range(1, FS):
-        feat_copy(i).wait_send()
-    for i in range(FS):
-
-        @pl.when(has_low)
-        def _():
-            halo_copy(i, 0).wait_send()
-
-        @pl.when(has_high)
-        def _():
-            halo_copy(i, 1).wait_send()
-
-    for direction in range(2):
-        for piece in range(2):
-            tok_first(direction, piece).wait_send()
-        tok_second(direction).wait_send()
-    for i in range(1, FS):
-        for piece in range(2):
-            tok_to_pair(fs_of(i), piece).wait_send()
+    drain(sbuf.at[1:FS], feat_sent)
+
+    @pl.when(has_low)
+    def _():
+        drain(kvg.at[:, 0:144], halo_sent[0])
+
+    @pl.when(has_high)
+    def _():
+        drain(kvg.at[:, 144:288], halo_sent[1])
+
+    drain(tok.at[0:3], tok_sent)
     end_gather(gather_in)
     end_gather(gather_out)
 
@@ -575,14 +643,31 @@
     w_conv_out,
 ):
     vmem = pl.BlockSpec(memory_space=pltpu.VMEM)
-    smem = pl.BlockSpec(memory_space=pltpu.SMEM)
+    anywhere = pl.BlockSpec(memory_space=pl.ANY)
     dma = pltpu.SemaphoreType.DMA
+    args = (
+        tokens,
+        norm_gain.reshape(1, -1),
+        w_query,
+        w_key,
+        w_value,
+        w_conv_in,
+        w_conv_gate,
+        sink_logit.reshape(1, -1),
+        conv_taps,
+        conv_bias.reshape(1, -1),
+        channel_gain.reshape(1, -1),
+        channel_shift.reshape(1, -1),
+        w_attn_out.T,
+        w_conv_out.T,
+    )
     return pl.pallas_call(
         kernel,
         out_shape=jax.ShapeDtypeStruct((HALF, D), BF16),
-        in_specs=[vmem] * 7 + [smem] + [vmem] * 6,
+        in_specs=[anywhere] * len(args),
         out_specs=vmem,
-        scratch_shapes=[
+        scratch_shapes=[pltpu.VMEM(a.shape, a.dtype) for a in args]
+        + [
             pltpu.VMEM((FS, TOK, D), BF16),
             pltpu.VMEM((D, 512), BF16),
             pltpu.VMEM((D, 1024), BF16),
@@ -602,44 +687,23 @@
             pltpu.VMEM((D // CHUNK, HALF, CHUNK), F32),
             pltpu.VMEM((D // CHUNK, HALF, CHUNK), BF16),
             pltpu.VMEM((D // CHUNK, HALF, CHUNK), BF16),
-            dma((64,)),
+            dma((15,)),
             dma((RING,)),
-            dma((2, 64)),
-            dma((64,)),
+            dma((RING, 4)),
             dma((RING,)),
-            dma((2, 64)),
+            dma((RING, 4)),
             dma((FS, 2, 2)),
-            dma((2, 2)),
-            dma((2,)),
-            dma((FS, 2)),
-            dma((FS, 2)),
             dma((FS, 2)),
             dma((FS,)),
-            dma((FS,)),
-            dma((2,)),
+            dma((1,)),
             dma((D // CHUNK,)),
-            dma((D // CHUNK,)),
+            dma((8,)),
         ],
         compiler_params=pltpu.CompilerParams(
             collective_id=0, has_side_effects=True, vmem_limit_bytes=60 * 1024 * 1024
         ),
         name="fused",
-    )(
-        tokens,
-        norm_gain.reshape(1, -1),
-        w_query,
-        w_key,
-        w_value,
-        w_conv_in,
-        w_conv_gate,
-        sink_logit,
-        conv_taps,
-        conv_bias.reshape(1, -1),
-        channel_gain.reshape(1, -1),
-        channel_shift.reshape(1, -1),
-        w_attn_out,
-        w_conv_out,
-    )
+    )(*args)
 
 
 def solution(mesh):

time: 88.1 us -> 70.3 us (0.80)
  Pallas kernels: 83.4 us -> 68.3 us
  local copies, waits for them, and re-layouts: 4.43 us -> 1.88 us
    pallas_call x1, Pallas kernels: 83.4 us -> 68.3 us  [local(): pl.pallas_call(kernel, out_shape=jax.ShapeDtypeStruct((HALF, D), BF16), i...]
    unnamed x5 -> x1, local copies, waits for them, and re-layouts: 4.43 us -> 1.88 us
where the time goes in v2:
time: 70.3 us; the launch traced here: 70.1 us
  Pallas kernels  68.3 us (97%)
  local copies, waits for them, and re-layouts  1.88 us (3%)
    pallas_call x1, Pallas kernels, local(): pl.pallas_call(kernel, out_shape=jax.ShapeDtypeStruct((HALF, D), BF16), i...  68.3 us
    unnamed x1, local copies, waits for them, and re-layouts  1.88 us

profile of v2, /device:TPU:1, one launch (start us, length us, event | category | flops | bytes accessed | tf_op | source)
XLA Modules:
  0.0 70.1 jit_solution(5259728341789519009)
XLA Ops:
  0.0 68.3 %fused.1 = bf16[128,2048]{1,0:T(8,128)(2,1)} custom-call(bf16[256,2048]{1,0:T(8,128)(2,1)} %refs_0_.1, f32[1,2048]{1,0:T(1,128)} %bitcast.9, bf16[32,512]{1,0:T(8,128)(2,1)} %refs_2_.1, bf16[32,128]{1,0:T(8,128)(2,1)} %refs_3_.1, bf16[32,128]{1,0:T(8,128)(2,1)} %refs_4_.1, bf16[32,512]{1,0:T(8,128)(2,1)} %refs_5_.1, bf16[32,512]{1,0:T(8,128)(2,1)} %refs_6_.1, ...), custom_call_target="tpu_custom_call" | custom-call | tf_op jit(solution)/shard_map/fused/pallas_call | solution.py:664
  68.3 1.9 %copy.16 = bf16[128,2048]{1,0:T(8,128)(2,1)} copy(bf16[128,2048]{1,0:T(8,128)(2,1)} %fused.1) | data formatting | bytes 1048576

commit v3 on v2

--- a/solution.py
+++ b/solution.py
@@ -67,8 +67,10 @@
         gext,
         low,
         high,
-        sbuf,
-        feat,
+        sconv,
+        satt,
+        fconv,
+        fatt,
         raw,
         cvals,
         stat_out,
@@ -88,10 +90,10 @@
         part_recv,
         send_sem,
     ) = refs
-    in_sent, out_sent, tok_sent, feat_sent, stat_sent, part_sent = (
-        send_sem.at[k] for k in range(6)
+    in_sent, out_sent, tok_sent, conv_sent, att_sent, stat_sent, part_sent = (
+        send_sem.at[k] for k in range(7)
     )
-    halo_sent = (send_sem.at[6], send_sem.at[7])
+    halo_sent = (send_sem.at[7], send_sem.at[8])
     sp = lax.axis_index("sp")
     f = lax.axis_index("fs")
     c = lax.axis_index("tp")
@@ -329,8 +331,6 @@
     gather_out = (wout, out_recv_a, out_recv_b, out_sent)
     start_gather(gather_in, False)
 
-    load_other.wait()
-    norm_rows(pl.multiple_of(partner * HALF, HALF))
     for copy in load_out:
         copy.wait()
     for k in range(FS):
@@ -338,8 +338,11 @@
         wout[pl.ds(mine, 32), k * 256 : k * 256 + 128] = wao_ref[:, at]
         wout[pl.ds(mine, 32), k * 256 + 128 : (k + 1) * 256] = wco_ref[:, at]
 
+    start_gather(gather_out, True)
+    load_other.wait()
+    norm_rows(pl.multiple_of(partner * HALF, HALF))
     serve_a(gather_in, 1, 8, False)
-    start_gather(gather_out, True)
+    serve_a(gather_out, 1, 3, True)
     serve_b(gather_in, 1, 0, 4)
 
     lane = lax.broadcasted_iota(jnp.int32, (HALF, 128), 1)
@@ -360,9 +363,9 @@
     def _():
         high[...] = jnp.zeros_like(high)
 
-    serve_a(gather_out, 1, 3, True)
+    serve_a(gather_out, 3, 5, True)
     serve_b(gather_in, 2, 0, 4)
-    serve_a(gather_out, 3, 5, True)
+    serve_a(gather_out, 5, 7, True)
 
     for direction in range(2):
         slot = fs_of(3 - 2 * direction)
@@ -371,15 +374,18 @@
         tok_to_pair(slot, direction).start()
 
     serve_b(gather_in, 3, 0, 4)
-    serve_a(gather_out, 5, 7, True)
+    serve_a(gather_out, 7, 8, True)
 
     for direction in range(2):
         slot = fs_of(3 - 2 * direction)
         tok_to_pair(slot, 1 - direction).wait_recv()
         tok_to_pair(slot, 1 - direction).start()
 
+    serve_b(gather_out, 1, 0, 1)
     serve_b(gather_in, 4, 0, 4)
-    serve_a(gather_out, 7, 8, True)
+    for piece in range(2):
+        tok_to_pair(fs_of(2), piece).wait_recv()
+        tok_to_pair(fs_of(2), piece).start()
     for copy in load_rest:
         copy.wait()
 
@@ -442,14 +448,6 @@
     ]
 
     def mix(i):
-        @pl.when(has_low)
-        def _():
-            halo_copy(i, 1).wait_recv()
-
-        @pl.when(has_high)
-        def _():
-            halo_copy(i, 0).wait_recv()
-
         own_kv = kvg[i, 16:272]
         own_ones = jnp.where(
             lax.broadcasted_iota(jnp.int32, (TOK, 128), 1) < 64, jnp.ones_like(own_kv), own_kv
@@ -476,7 +474,16 @@
                 )
                 heads.append(mixed / (pltpu.roll(mixed, 64, 1) + jnp.exp(sink - top)))
             joined = jnp.where(half_lane < 64, pltpu.roll(heads[0], 64, 1), heads[1])
-            sbuf[i, block * HALF : (block + 1) * HALF, 0:128] = joined.astype(BF16)
+            satt[i, block * HALF : (block + 1) * HALF] = joined.astype(BF16)
+
+    def filter_taps(i):
+        @pl.when(has_low)
+        def _():
+            halo_copy(i, 1).wait_recv()
+
+        @pl.when(has_high)
+        def _():
+            halo_copy(i, 0).wait_recv()
 
         gext[i, 0:16] = low[i, 128:144].astype(F32)
         gext[i, 272:288] = high[i, 0:16].astype(F32)
@@ -486,66 +493,71 @@
             for k in range(TAPS):
                 at = block * 64 + k + 1
                 total = total + taps_ref[k : k + 1, cols] * gext[i, at : at + 64]
-            sbuf[i, block * 64 : (block + 1) * 64, 128:256] = total.astype(BF16)
-
-    def feat_copy(i):
+            sconv[i, block * 64 : (block + 1) * 64] = total.astype(BF16)
+
+    def feat_copy(kind, i):
         return pltpu.make_async_remote_copy(
-            src_ref=sbuf.at[i],
-            dst_ref=feat.at[f],
-            send_sem=feat_sent,
-            recv_sem=feat_recv.at[f],
+            src_ref=(sconv, satt)[kind].at[i],
+            dst_ref=(fconv, fatt)[kind].at[f],
+            send_sem=(conv_sent, att_sent)[kind],
+            recv_sem=feat_recv.at[kind, f],
             device_id={"fs": fs_of(i)},
             device_id_type=MESH,
         )
+
+    def feat_wait(kind, src):
+        pltpu.make_async_remote_copy(
+            src_ref=(sconv, satt)[kind].at[0],
+            dst_ref=(fconv, fatt)[kind].at[src],
+            send_sem=(conv_sent, att_sent)[kind],
+            recv_sem=feat_recv.at[kind, src],
+            device_id={"tp": partner},
+            device_id_type=MESH,
+        ).wait_recv()
 
     def wait_pair(slot):
         tok_copy(slot, partner, 0, tp=partner).wait_recv()
         tok_copy(slot, partner, 1, tp=partner).wait_recv()
 
-    project(0)
-    serve_b(gather_out, 1, 0, 1)
+    serve_b(gather_out, 1, 1, 3)
     wait_pair(fs_of(1))
     project(1)
-    serve_b(gather_out, 1, 1, 2)
     wait_pair(fs_of(3))
     project(3)
-    for piece in range(2):
-        tok_to_pair(fs_of(2), piece).wait_recv()
-        tok_to_pair(fs_of(2), piece).start()
-    serve_b(gather_out, 1, 2, 3)
-    mix(0)
-    feat[f] = sbuf[0]
     serve_b(gather_out, 1, 3, 4)
     wait_pair(fs_of(2))
     project(2)
     serve_b(gather_out, 2, 0, 1)
+    project(0)
+    serve_b(gather_out, 2, 1, 4)
+    filter_taps(1)
+    feat_copy(0, 1).start()
+    filter_taps(3)
+    feat_copy(0, 3).start()
+    serve_b(gather_out, 3, 0, 1)
+    filter_taps(2)
+    feat_copy(0, 2).start()
+    filter_taps(0)
+    fconv[f] = sconv[0]
+    serve_b(gather_out, 3, 1, 2)
+    mix(2)
+    feat_copy(1, 2).start()
+    serve_b(gather_out, 3, 2, 3)
     mix(1)
-    feat_copy(1).start()
-    serve_b(gather_out, 2, 1, 3)
+    feat_copy(1, 1).start()
+    serve_b(gather_out, 3, 3, 4)
     mix(3)
-    feat_copy(3).start()
-    serve_b(gather_out, 2, 3, 4)
-    serve_b(gather_out, 3, 0, 1)
-    mix(2)
-    feat_copy(2).start()
-    serve_b(gather_out, 3, 1, 4)
-
-    def feat_wait(src):
-        pltpu.make_async_remote_copy(
-            src_ref=sbuf.at[0],
-            dst_ref=feat.at[src],
-            send_sem=feat_sent,
-            recv_sem=feat_recv.at[src],
-            device_id={"tp": partner},
-            device_id_type=MESH,
-        ).wait_recv()
-
-    for i in (1, 3, 2):
-        feat_wait(fs_of(i))
+    feat_copy(1, 3).start()
+
+    for i in range(1, FS):
+        feat_wait(0, fs_of(i))
 
     total = jnp.zeros((TOK, 1), F32)
     for k in range(FS):
-        values = feat[k, :, 128:256].astype(F32) + bias_ref[:, k * 128 : (k + 1) * 128]
+        values = jnp.concatenate(
+            [fconv[k, other_half], fconv[k, own_half]], axis=0
+        ).astype(F32)
+        values = values + bias_ref[:, k * 128 : (k + 1) * 128]
         cvals[:, k * 128 : (k + 1) * 128] = values
         total = total + jnp.sum(values, axis=-1, keepdims=True)
     here = total / 512.0
@@ -563,18 +575,25 @@
         device_id_type=MESH,
     )
     stat_copy.start()
-    for k in range(FS):
-        raw[:, k * 256 : k * 256 + 128] = feat[k, :, 0:128]
+    mix(0)
+    fatt[f] = satt[0]
     stat_copy.wait_recv()
-    there = stat_in[:, 0:1]
+    swapped = jnp.concatenate([stat_in[HALF:TOK, :], stat_in[0:HALF, :]], axis=0)
+    there = swapped[:, 0:1]
     gap = here - there
     centre = 0.5 * (here + there)
-    spread = (around + stat_in[:, 64:65] + 256.0 * gap * gap) / 1024.0
+    spread = (around + swapped[:, 64:65] + 256.0 * gap * gap) / 1024.0
     scale = lax.rsqrt(spread + EPSILON)
     for k in range(FS):
         at = slice(k * 128, (k + 1) * 128)
         v = (cvals[:, at] - centre) * scale * cgain_ref[:, at] + cshift_ref[:, at]
         raw[:, k * 256 + 128 : (k + 1) * 256] = (v / (1.0 + jnp.exp(-v))).astype(BF16)
+
+    for i in range(1, FS):
+        feat_wait(1, fs_of(i))
+    for k in range(FS):
+        raw[0:HALF, k * 256 : k * 256 + 128] = fatt[k, other_half]
+        raw[HALF:TOK, k * 256 : k * 256 + 128] = fatt[k, own_half]
 
     serve_b(gather_out, 4, 0, 4)
 
@@ -590,11 +609,10 @@
 
     for n in range(D // CHUNK):
         weights = wout[n * CHUNK : (n + 1) * CHUNK, :]
-        part_out[n] = lax.dot_general(
-            raw[other_half, :], weights, NT, preferred_element_type=F32
-        ).astype(BF16)
+        product = lax.dot_general(raw[...], weights, NT, preferred_element_type=F32)
+        part_out[n] = product[0:HALF].astype(BF16)
         part_copy(n).start()
-        part[n] = lax.dot_general(raw[own_half, :], weights, NT, preferred_element_type=F32)
+        part[n] = product[HALF:TOK]
     for n in range(D // CHUNK):
         part_copy(n).wait_recv()
         out_ref[:, n * CHUNK : (n + 1) * CHUNK] = (part[n] + part_in[n].astype(F32)).astype(BF16)
@@ -611,7 +629,8 @@
 
     drain(part_out, part_sent)
     stat_copy.wait_send()
-    drain(sbuf.at[1:FS], feat_sent)
+    drain(sconv.at[1:FS], conv_sent)
+    drain(satt.at[1:FS], att_sent)
 
     @pl.when(has_low)
     def _():
@@ -678,8 +697,10 @@
             pltpu.VMEM((FS, 288, 128), F32),
             pltpu.VMEM((FS, 144, 128), BF16),
             pltpu.VMEM((FS, 144, 128), BF16),
-            pltpu.VMEM((FS, TOK, 256), BF16),
-            pltpu.VMEM((FS, TOK, 256), BF16),
+            pltpu.VMEM((FS, TOK, 128), BF16),
+            pltpu.VMEM((FS, TOK, 128), BF16),
+            pltpu.VMEM((FS, TOK, 128), BF16),
+            pltpu.VMEM((FS, TOK, 128), BF16),
             pltpu.VMEM((TOK, 1024), BF16),
             pltpu.VMEM((TOK, 512), F32),
             pltpu.VMEM((TOK, 128), F32),
@@ -694,10 +715,10 @@
             dma((RING, 4)),
             dma((FS, 2, 2)),
             dma((FS, 2)),
-            dma((FS,)),
+            dma((2, FS)),
             dma((1,)),
             dma((D // CHUNK,)),
-            dma((8,)),
+            dma((9,)),
         ],
         compiler_params=pltpu.CompilerParams(
             collective_id=0, has_side_effects=True, vmem_limit_bytes=60 * 1024 * 1024

time: 70.3 us -> 66.3 us (0.943)
  Pallas kernels: 68.3 us -> 64.3 us
    pallas_call x1, Pallas kernels: 68.3 us -> 64.3 us  [local(): pl.pallas_call(kernel, out_shape=jax.ShapeDtypeStruct((HALF, D), BF16), i...]
where the time goes in v3:
time: 66.3 us; the launch traced here: 66.1 us
  Pallas kernels  64.3 us (97%)
  local copies, waits for them, and re-layouts  1.88 us (3%)
    pallas_call x1, Pallas kernels, local(): pl.pallas_call(kernel, out_shape=jax.ShapeDtypeStruct((HALF, D), BF16), i...  64.3 us
    unnamed x1, local copies, waits for them, and re-layouts  1.88 us

profile of v3, /device:TPU:1, one launch (start us, length us, event | category | flops | bytes accessed | tf_op | source)
XLA Modules:
  0.0 66.1 jit_solution(14517770076458899996)
XLA Ops:
  0.0 64.3 %fused.1 = bf16[128,2048]{1,0:T(8,128)(2,1)} custom-call(bf16[256,2048]{1,0:T(8,128)(2,1)} %refs_0_.1, f32[1,2048]{1,0:T(1,128)} %bitcast.9, bf16[32,512]{1,0:T(8,128)(2,1)} %refs_2_.1, bf16[32,128]{1,0:T(8,128)(2,1)} %refs_3_.1, bf16[32,128]{1,0:T(8,128)(2,1)} %refs_4_.1, bf16[32,512]{1,0:T(8,128)(2,1)} %refs_5_.1, bf16[32,512]{1,0:T(8,128)(2,1)} %refs_6_.1, ...), custom_call_target="tpu_custom_call" | custom-call | tf_op jit(solution)/shard_map/fused/pallas_call | solution.py:683
  64.3 1.9 %copy.16 = bf16[128,2048]{1,0:T(8,128)(2,1)} copy(bf16[128,2048]{1,0:T(8,128)(2,1)} %fused.1) | data formatting | bytes 1048576

commit v4 on v3

--- a/solution.py
+++ b/solution.py
@@ -184,10 +184,6 @@
 
         lax.fori_loop(0, HALF // 16, body, 0)
 
-    for copy in load_own:
-        copy.wait()
-    norm_rows(pl.multiple_of(c * HALF, HALF))
-
     pl.semaphore_wait(barrier, RING - 1 + 2 + FS - 1 + 1 + 2)
 
     def tok_rows(half, piece):
@@ -213,10 +209,6 @@
 
     def tok_to_pair(slot, piece):
         return tok_copy(slot, c, piece, tp=partner)
-
-    for first in range(2):
-        for direction in range(2):
-            tok_first(direction, (first + direction) % 2).start()
 
     def slab(buf, index):
         return buf.at[pl.ds(pl.multiple_of(index * 32, 32), 32)]
@@ -264,7 +256,7 @@
         b_copy(gather, 1, 0, me_b).start()
 
         def body(step, carry):
-            a_copy(gather, me_a, step).start()
+            a_copy(gather, me_a, 4 + (step // 2) * (2 * (step % 2) - 1)).start()
             return carry
 
         if relay:
@@ -330,6 +322,12 @@
     gather_in = (win, in_recv_a, in_recv_b, in_sent)
     gather_out = (wout, out_recv_a, out_recv_b, out_sent)
     start_gather(gather_in, False)
+    for copy in load_own:
+        copy.wait()
+    norm_rows(pl.multiple_of(c * HALF, HALF))
+    for first in range(2):
+        for direction in range(2):
+            tok_first(direction, (first + direction) % 2).start()
 
     for copy in load_out:
         copy.wait()
@@ -341,10 +339,6 @@
     start_gather(gather_out, True)
     load_other.wait()
     norm_rows(pl.multiple_of(partner * HALF, HALF))
-    serve_a(gather_in, 1, 8, False)
-    serve_a(gather_out, 1, 3, True)
-    serve_b(gather_in, 1, 0, 4)
-
     lane = lax.broadcasted_iota(jnp.int32, (HALF, 128), 1)
     frequency = jnp.exp((lane % 16).astype(F32) * (-math.log(ROPE_BASE) / 16))
     for k in range(2):
@@ -363,6 +357,10 @@
     def _():
         high[...] = jnp.zeros_like(high)
 
+    serve_a(gather_in, 1, 8, False)
+    serve_a(gather_out, 1, 3, True)
+    serve_b(gather_in, 1, 0, 4)
+
     serve_a(gather_out, 3, 5, True)
     serve_b(gather_in, 2, 0, 4)
     serve_a(gather_out, 5, 7, True)
@@ -381,13 +379,13 @@
         tok_to_pair(slot, 1 - direction).wait_recv()
         tok_to_pair(slot, 1 - direction).start()
 
-    serve_b(gather_out, 1, 0, 1)
+    serve_b(gather_out, 1, 0, 2)
     serve_b(gather_in, 4, 0, 4)
+    for copy in load_rest:
+        copy.wait()
     for piece in range(2):
         tok_to_pair(fs_of(2), piece).wait_recv()
         tok_to_pair(fs_of(2), piece).start()
-    for copy in load_rest:
-        copy.wait()
 
     def halo_copy(i, side):
         at = side * 144
@@ -411,8 +409,11 @@
         acc = jnp.dot(tok[slot], win[...], preferred_element_type=F32)
         cosine, sine = ctab[...], stab[...]
         query = rotated(acc[:, 0:128], cosine, sine).astype(BF16).astype(F32) * HEAD_DIM**-0.5
-        qbuf[i, 0] = jnp.where(lanes < 64, query, 0.0).astype(BF16)
-        qbuf[i, 1] = jnp.where(lanes < 64, pltpu.roll(query, 64, 1), 0.0).astype(BF16)
+        for h in range(2):
+            head = query if h == 0 else pltpu.roll(query, 64, 1)
+            head = jnp.where(lanes < 64, head, 0.0).astype(BF16)
+            for block in range(2):
+                qbuf[i, block, h * HALF : (h + 1) * HALF] = head[block * HALF : (block + 1) * HALF]
         pair = acc[:, 128:256]
         turned = rotated(pair, cosine, sine)
         kvg[i, 16:272] = jnp.where(lanes < 64, turned, pair).astype(BF16)
@@ -429,51 +430,45 @@
         def _():
             halo_copy(i, 1).start()
 
-    row_at = lax.broadcasted_iota(jnp.int32, (HALF, 256), 0)
-    key_at = lax.broadcasted_iota(jnp.int32, (HALF, 256), 1)
-    half_row = lax.broadcasted_iota(jnp.int32, (HALF, 128), 0)
-    half_key = lax.broadcasted_iota(jnp.int32, (HALF, 128), 1)
-    half_lane = half_key
+    row_at = lax.broadcasted_iota(jnp.int32, (TOK, TOK), 0) % HALF
+    key_at = lax.broadcasted_iota(jnp.int32, (TOK, TOK), 1)
+    half_row = lax.broadcasted_iota(jnp.int32, (TOK, HALF), 0) % HALF
+    half_key = lax.broadcasted_iota(jnp.int32, (TOK, HALF), 1)
+    half_lane = lax.broadcasted_iota(jnp.int32, (HALF, 128), 1)
     far = RING * TOK
     own_valid = (key_at - row_at <= WINDOW, key_at >= row_at)
     halo_valid = (
         half_key >= half_row + jnp.where(has_low, 0, far),
         half_key + jnp.where(has_high, 0, far) <= half_row,
     )
-
     head_lane = lax.broadcasted_iota(jnp.int32, (1, 8), 1)
     sinks = [
         jnp.sum(jnp.where(head_lane == 2 * f + h, sink_ref[...], 0.0), axis=-1, keepdims=True)
         for h in range(2)
     ]
+    first_head = lax.broadcasted_iota(jnp.int32, (TOK, 1), 0) < HALF
+    sink = jnp.where(first_head, sinks[0], sinks[1])
 
     def mix(i):
         own_kv = kvg[i, 16:272]
-        own_ones = jnp.where(
-            lax.broadcasted_iota(jnp.int32, (TOK, 128), 1) < 64, jnp.ones_like(own_kv), own_kv
-        )
+        own_ones = jnp.where(lanes < 64, jnp.ones_like(own_kv), own_kv)
         for block in range(2):
             near_kv = low[i, 0:128] if block == 0 else high[i, 16:144]
             near_ones = jnp.where(half_lane < 64, jnp.ones_like(near_kv), near_kv)
-            heads = []
-            for h in range(2):
-                q = qbuf[i, h, block * HALF : (block + 1) * HALF]
-                s_own = lax.dot_general(q, own_kv, NT, preferred_element_type=F32)
-                s_near = lax.dot_general(q, near_kv, NT, preferred_element_type=F32)
-                s_own = jnp.where(own_valid[block], s_own, NEGATIVE)
-                s_near = jnp.where(halo_valid[block], s_near, NEGATIVE)
-                sink = sinks[h]
-                top = jnp.maximum(
-                    jnp.maximum(s_own[:, 0:128], s_own[:, 128:256]), s_near
-                )
-                top = jnp.maximum(jnp.max(top, axis=-1, keepdims=True), sink)
-                p_own = jnp.exp(s_own - top).astype(BF16)
-                p_near = jnp.exp(s_near - top).astype(BF16)
-                mixed = jnp.dot(p_own, own_ones, preferred_element_type=F32) + jnp.dot(
-                    p_near, near_ones, preferred_element_type=F32
-                )
-                heads.append(mixed / (pltpu.roll(mixed, 64, 1) + jnp.exp(sink - top)))
-            joined = jnp.where(half_lane < 64, pltpu.roll(heads[0], 64, 1), heads[1])
+            q = qbuf[i, block]
+            s_own = lax.dot_general(q, own_kv, NT, preferred_element_type=F32)
+            s_near = lax.dot_general(q, near_kv, NT, preferred_element_type=F32)
+            s_own = jnp.where(own_valid[block], s_own, NEGATIVE)
+            s_near = jnp.where(halo_valid[block], s_near, NEGATIVE)
+            top = jnp.maximum(jnp.maximum(s_own[:, 0:128], s_own[:, 128:256]), s_near)
+            top = jnp.maximum(jnp.max(top, axis=-1, keepdims=True), sink)
+            p_own = jnp.exp(s_own - top).astype(BF16)
+            p_near = jnp.exp(s_near - top).astype(BF16)
+            mixed = jnp.dot(p_own, own_ones, preferred_element_type=F32) + jnp.dot(
+                p_near, near_ones, preferred_element_type=F32
+            )
+            mixed = mixed / (pltpu.roll(mixed, 64, 1) + jnp.exp(sink - top))
+            joined = jnp.where(half_lane < 64, pltpu.roll(mixed[0:HALF], 64, 1), mixed[HALF:TOK])
             satt[i, block * HALF : (block + 1) * HALF] = joined.astype(BF16)
 
     def filter_taps(i):
@@ -519,9 +514,9 @@
         tok_copy(slot, partner, 0, tp=partner).wait_recv()
         tok_copy(slot, partner, 1, tp=partner).wait_recv()
 
-    serve_b(gather_out, 1, 1, 3)
     wait_pair(fs_of(1))
     project(1)
+    serve_b(gather_out, 1, 2, 3)
     wait_pair(fs_of(3))
     project(3)
     serve_b(gather_out, 1, 3, 4)
@@ -529,25 +524,26 @@
     project(2)
     serve_b(gather_out, 2, 0, 1)
     project(0)
-    serve_b(gather_out, 2, 1, 4)
+    serve_b(gather_out, 2, 1, 2)
     filter_taps(1)
     feat_copy(0, 1).start()
+    serve_b(gather_out, 2, 2, 3)
     filter_taps(3)
     feat_copy(0, 3).start()
-    serve_b(gather_out, 3, 0, 1)
+    serve_b(gather_out, 2, 3, 4)
     filter_taps(2)
     feat_copy(0, 2).start()
+    mix(1)
+    feat_copy(1, 1).start()
+    serve_b(gather_out, 3, 0, 1)
+    mix(2)
+    feat_copy(1, 2).start()
+    serve_b(gather_out, 3, 1, 2)
+    mix(3)
+    feat_copy(1, 3).start()
+    serve_b(gather_out, 3, 2, 3)
     filter_taps(0)
     fconv[f] = sconv[0]
-    serve_b(gather_out, 3, 1, 2)
-    mix(2)
-    feat_copy(1, 2).start()
-    serve_b(gather_out, 3, 2, 3)
-    mix(1)
-    feat_copy(1, 1).start()
-    serve_b(gather_out, 3, 3, 4)
-    mix(3)
-    feat_copy(1, 3).start()
 
     for i in range(1, FS):
         feat_wait(0, fs_of(i))
@@ -575,6 +571,7 @@
         device_id_type=MESH,
     )
     stat_copy.start()
+    serve_b(gather_out, 3, 3, 4)
     mix(0)
     fatt[f] = satt[0]
     stat_copy.wait_recv()
@@ -721,10 +718,10 @@
             dma((9,)),
         ],
         compiler_params=pltpu.CompilerParams(
-            collective_id=0, has_side_effects=True, vmem_limit_bytes=60 * 1024 * 1024
+            collective_id=0, has_side_effects=True, vmem_limit_bytes=32 * 1024 * 1024
         ),
         name="fused",
-    )(*args)
+    )(*(pltpu.with_memory_space_constraint(a, pltpu.HBM) for a in args))
 
 
 def solution(mesh):

time: 66.3 us -> 64.1 us (0.967)
  Pallas kernels: 64.3 us -> 63.1 us
  local copies, waits for them, and re-layouts: 1.88 us -> 0.8 us
    pallas_call x1, Pallas kernels: 64.3 us -> 63.1 us  [local(): pl.pallas_call(kernel, out_shape=jax.ShapeDtypeStruct((HALF, D), BF16), i...]
    unnamed x1, local copies, waits for them, and re-layouts: 1.88 us -> 0.8 us
where the time goes in v4:
time: 64.1 us; the launch traced here: 64 us
  Pallas kernels  63.1 us (98%)
  local copies, waits for them, and re-layouts  0.8 us (1%)
    pallas_call x1, Pallas kernels, local(): pl.pallas_call(kernel, out_shape=jax.ShapeDtypeStruct((HALF, D), BF16), i...  63.1 us

profile of v4, /device:TPU:1, one launch (start us, length us, event | category | flops | bytes accessed | tf_op | source)
XLA Modules:
  0.0 64.0 jit_solution(829185133533684760)
XLA Ops:
  0.0 63.1 %fused.1 = bf16[128,2048]{1,0:T(8,128)(2,1)S(1)} custom-call(bf16[256,2048]{1,0:T(8,128)(2,1)} %refs_0_.1, f32[1,2048]{1,0:T(1,128)} %bitcast.9, bf16[32,512]{1,0:T(8,128)(2,1)} %refs_2_.1, bf16[32,128]{1,0:T(8,128)(2,1)} %refs_3_.1, bf16[32,128]{1,0:T(8,128)(2,1)} %refs_4_.1, bf16[32,512]{1,0:T(8,128)(2,1)} %refs_5_.1, bf16[32,512]{1,0:T(8,128)(2,1)} %refs_6_.1, ...), custom_call_target="tpu_custom_call" | custom-call | tf_op jit(solution)/shard_map/fused/pallas_call | solution.py:680
  63.2 0.8 %copy.16 = bf16[128,2048]{1,0:T(8,128)(2,1)} copy(bf16[128,2048]{1,0:T(8,128)(2,1)S(1)} %fused.1) | data formatting | bytes 1048576

commit v5 on v4

--- a/solution.py
+++ b/solution.py
@@ -255,15 +255,12 @@
         b_copy(gather, 0, 0, me_b).start()
         b_copy(gather, 1, 0, me_b).start()
 
-        def body(step, carry):
-            a_copy(gather, me_a, 4 + (step // 2) * (2 * (step % 2) - 1)).start()
-            return carry
-
         if relay:
             a_copy(gather, me_a, 1).start()
             a_copy(gather, me_a, -1).start()
         else:
-            lax.fori_loop(1, RING, body, 0)
+            for step in (1, -1, 4, 3, -3, 2, -2):
+                a_copy(gather, me_a, step).start()
 
     def serve_a(gather, first, last, relay):
         def body(j, carry):
@@ -379,13 +376,13 @@
         tok_to_pair(slot, 1 - direction).wait_recv()
         tok_to_pair(slot, 1 - direction).start()
 
-    serve_b(gather_out, 1, 0, 2)
+    serve_b(gather_out, 1, 0, 3)
+    for piece in range(2):
+        tok_to_pair(fs_of(2), piece).wait_recv()
+        tok_to_pair(fs_of(2), piece).start()
     serve_b(gather_in, 4, 0, 4)
     for copy in load_rest:
         copy.wait()
-    for piece in range(2):
-        tok_to_pair(fs_of(2), piece).wait_recv()
-        tok_to_pair(fs_of(2), piece).start()
 
     def halo_copy(i, side):
         at = side * 144
@@ -516,26 +513,23 @@
 
     wait_pair(fs_of(1))
     project(1)
-    serve_b(gather_out, 1, 2, 3)
+    serve_b(gather_out, 1, 3, 4)
     wait_pair(fs_of(3))
     project(3)
-    serve_b(gather_out, 1, 3, 4)
     wait_pair(fs_of(2))
     project(2)
     serve_b(gather_out, 2, 0, 1)
     project(0)
-    serve_b(gather_out, 2, 1, 2)
+    serve_b(gather_out, 2, 1, 4)
     filter_taps(1)
     feat_copy(0, 1).start()
-    serve_b(gather_out, 2, 2, 3)
     filter_taps(3)
     feat_copy(0, 3).start()
-    serve_b(gather_out, 2, 3, 4)
-    filter_taps(2)
-    feat_copy(0, 2).start()
     mix(1)
     feat_copy(1, 1).start()
     serve_b(gather_out, 3, 0, 1)
+    filter_taps(2)
+    feat_copy(0, 2).start()
     mix(2)
     feat_copy(1, 2).start()
     serve_b(gather_out, 3, 1, 2)
@@ -544,6 +538,7 @@
     serve_b(gather_out, 3, 2, 3)
     filter_taps(0)
     fconv[f] = sconv[0]
+    serve_b(gather_out, 3, 3, 4)
 
     for i in range(1, FS):
         feat_wait(0, fs_of(i))
@@ -571,7 +566,6 @@
         device_id_type=MESH,
     )
     stat_copy.start()
-    serve_b(gather_out, 3, 3, 4)
     mix(0)
     fatt[f] = satt[0]
     stat_copy.wait_recv()

time: 64.1 us -> 63.4 us (0.989)
    pallas_call x1, Pallas kernels: 63.1 us -> 62.5 us  [local(): pl.pallas_call(kernel, out_shape=jax.ShapeDtypeStruct((HALF, D), BF16), i...]
where the time goes in v5:
time: 63.4 us; the launch traced here: 63.3 us
  Pallas kernels  62.5 us (99%)
  local copies, waits for them, and re-layouts  0.8 us (1%)
    pallas_call x1, Pallas kernels, local(): pl.pallas_call(kernel, out_shape=jax.ShapeDtypeStruct((HALF, D), BF16), i...  62.5 us

profile of v5, /device:TPU:1, one launch (start us, length us, event | category | flops | bytes accessed | tf_op | source)
XLA Modules:
  0.0 63.3 jit_solution(4349422145348115683)
XLA Ops:
  0.0 62.5 %fused.1 = bf16[128,2048]{1,0:T(8,128)(2,1)S(1)} custom-call(bf16[256,2048]{1,0:T(8,128)(2,1)} %refs_0_.1, f32[1,2048]{1,0:T(1,128)} %bitcast.9, bf16[32,512]{1,0:T(8,128)(2,1)} %refs_2_.1, bf16[32,128]{1,0:T(8,128)(2,1)} %refs_3_.1, bf16[32,128]{1,0:T(8,128)(2,1)} %refs_4_.1, bf16[32,512]{1,0:T(8,128)(2,1)} %refs_5_.1, bf16[32,512]{1,0:T(8,128)(2,1)} %refs_6_.1, ...), custom_call_target="tpu_custom_call" | custom-call | tf_op jit(solution)/shard_map/fused/pallas_call | solution.py:674
  62.5 0.8 %copy.16 = bf16[128,2048]{1,0:T(8,128)(2,1)} copy(bf16[128,2048]{1,0:T(8,128)(2,1)S(1)} %fused.1) | data formatting | bytes 1048576

commit v6 on v5

--- a/solution.py
+++ b/solution.py
@@ -19,7 +19,7 @@
 TAPS = 31
 RING = 8
 FS = 4
-CHUNK = 512
+CHUNK = 1024
 MESH = pl.DeviceIdType.MESH
 NT = (((1,), (1,)), ((), ()))
 F32 = jnp.float32
@@ -319,6 +319,14 @@
     gather_in = (win, in_recv_a, in_recv_b, in_sent)
     gather_out = (wout, out_recv_a, out_recv_b, out_sent)
     start_gather(gather_in, False)
+    for copy in load_out:
+        copy.wait()
+    for k in range(FS):
+        at = pl.ds(pl.multiple_of(c * 512 + k * 128, 128), 128)
+        wout[pl.ds(mine, 32), k * 256 : k * 256 + 128] = wao_ref[:, at]
+        wout[pl.ds(mine, 32), k * 256 + 128 : (k + 1) * 256] = wco_ref[:, at]
+
+    start_gather(gather_out, True)
     for copy in load_own:
         copy.wait()
     norm_rows(pl.multiple_of(c * HALF, HALF))
@@ -326,14 +334,6 @@
         for direction in range(2):
             tok_first(direction, (first + direction) % 2).start()
 
-    for copy in load_out:
-        copy.wait()
-    for k in range(FS):
-        at = pl.ds(pl.multiple_of(c * 512 + k * 128, 128), 128)
-        wout[pl.ds(mine, 32), k * 256 : k * 256 + 128] = wao_ref[:, at]
-        wout[pl.ds(mine, 32), k * 256 + 128 : (k + 1) * 256] = wco_ref[:, at]
-
-    start_gather(gather_out, True)
     load_other.wait()
     norm_rows(pl.multiple_of(partner * HALF, HALF))
     lane = lax.broadcasted_iota(jnp.int32, (HALF, 128), 1)

time: 63.4 us -> 63.1 us (level)
  no operation moved by 1% of the time
where the time goes in v6:
time: 63.1 us; the launch traced here: 63 us
  Pallas kernels  62.2 us (99%)
  local copies, waits for them, and re-layouts  0.8 us (1%)
    pallas_call x1, Pallas kernels, local(): pl.pallas_call(kernel, out_shape=jax.ShapeDtypeStruct((HALF, D), BF16), i...  62.2 us

profile of v6, /device:TPU:1, one launch (start us, length us, event | category | flops | bytes accessed | tf_op | source)
XLA Modules:
  0.0 63.0 jit_solution(10021609099713561578)
XLA Ops:
  0.0 62.2 %fused.1 = bf16[128,2048]{1,0:T(8,128)(2,1)S(1)} custom-call(bf16[256,2048]{1,0:T(8,128)(2,1)} %refs_0_.1, f32[1,2048]{1,0:T(1,128)} %bitcast.9, bf16[32,512]{1,0:T(8,128)(2,1)} %refs_2_.1, bf16[32,128]{1,0:T(8,128)(2,1)} %refs_3_.1, bf16[32,128]{1,0:T(8,128)(2,1)} %refs_4_.1, bf16[32,512]{1,0:T(8,128)(2,1)} %refs_5_.1, bf16[32,512]{1,0:T(8,128)(2,1)} %refs_6_.1, ...), custom_call_target="tpu_custom_call" | custom-call | tf_op jit(solution)/shard_map/fused/pallas_call | solution.py:674
  62.2 0.8 %copy.16 = bf16[128,2048]{1,0:T(8,128)(2,1)} copy(bf16[128,2048]{1,0:T(8,128)(2,1)S(1)} %fused.1) | data formatting | bytes 1048576

commit v7 on v6

--- a/solution.py
+++ b/solution.py
@@ -391,7 +391,7 @@
             dst_ref=(low if side else high).at[i],
             send_sem=halo_sent[side],
             recv_sem=halo_recv.at[i, side],
-            device_id={"sp": sp + 2 * side - 1},
+            device_id={"sp": (sp + RING * RING + 2 * side - 1) % (RING * RING)},
             device_id_type=MESH,
         )
 

time: 63.1 us -> 63.1 us (level)
  no operation moved by 1% of the time
where the time goes in v7:
time: 63.1 us; the launch traced here: 63 us
  Pallas kernels  62.2 us (99%)
  local copies, waits for them, and re-layouts  0.8 us (1%)
    pallas_call x1, Pallas kernels, local(): pl.pallas_call(kernel, out_shape=jax.ShapeDtypeStruct((HALF, D), BF16), i...  62.2 us

profile of v7, /device:TPU:1, one launch (start us, length us, event | category | flops | bytes accessed | tf_op | source)
XLA Modules:
  0.0 63.0 jit_solution(7296129923242659404)
XLA Ops:
  0.0 62.2 %fused.1 = bf16[128,2048]{1,0:T(8,128)(2,1)S(1)} custom-call(bf16[256,2048]{1,0:T(8,128)(2,1)} %refs_0_.1, f32[1,2048]{1,0:T(1,128)} %bitcast.9, bf16[32,512]{1,0:T(8,128)(2,1)} %refs_2_.1, bf16[32,128]{1,0:T(8,128)(2,1)} %refs_3_.1, bf16[32,128]{1,0:T(8,128)(2,1)} %refs_4_.1, bf16[32,512]{1,0:T(8,128)(2,1)} %refs_5_.1, bf16[32,512]{1,0:T(8,128)(2,1)} %refs_6_.1, ...), custom_call_target="tpu_custom_call" | custom-call | tf_op jit(solution)/shard_map/fused/pallas_call | solution.py:674
  62.2 0.8 %copy.16 = bf16[128,2048]{1,0:T(8,128)(2,1)} copy(bf16[128,2048]{1,0:T(8,128)(2,1)S(1)} %fused.1) | data formatting | bytes 1048576
